TPU v7x, 32 devices: a whole 2x2x4 slice. The times are simulated.
32 devices in a mesh: sp: 8 (over z, x), tp: 4 (over y, core).
Axes of the slice: x: 2, y: 2, z: 4, core: 2. Of those that a mesh axis runs over, the one named last changes fastest.
Arguments:
- query_rows: bfloat16 [4096, 1024], P('sp', 'tp'), may hold values from -6 to 6
- key_rows: bfloat16 [4096, 1024], P('sp', 'tp'), may hold values from -6 to 6
- value_rows: bfloat16 [4096, 2048], P('sp', 'tp'), may hold values from -6 to 6
- out_gate_pre: bfloat16 [4096, 2048], P('sp', 'tp'), may hold values from -8 to 8
- input_gate_pre: float32 [4, 4096], P('tp', 'sp'), may hold values from -8 to 8
- forget_gate_pre: float32 [4, 4096], P('tp', 'sp'), may hold values from -26 to 26
- residual: bfloat16 [4096, 2048], P(('sp', 'tp')), may hold values from -6 to 6
- out_proj: bfloat16 [2048, 2048], P('tp'), may hold values from -0.125 to 0.125
- mix_gain: float32 [2048], replicated, may hold values from 0.1 to 1.9
- pre_gain: float32 [2048], replicated, may hold values from 0.1 to 1.9
- gate_proj: bfloat16 [2048, 3072], P('sp', 'tp'), may hold values from -0.125 to 0.125
- value_proj: bfloat16 [2048, 3072], P('sp', 'tp'), may hold values from -0.125 to 0.125
- gate_kernel: float32 [3, 3072], P(None, 'tp'), may hold values from -3.5 to 3.5
- value_kernel: float32 [3, 3072], P(None, 'tp'), may hold values from -3.5 to 3.5
- down_proj: bfloat16 [2048, 3072], P('sp', 'tp'), may hold values from -0.109375 to 0.109375
- post_gain: float32 [2048], replicated, may hold values from 0.1 to 1.9
Outputs:
- result: bfloat16 [4096, 2048], P(('sp', 'tp'))
All inputs are finite; a program needn't handle non-finite values.
Results may differ from a plain program's by a relative error of at most 0.017.
Values may be sent and summed in bfloat16 or wider, within the bound.
No kernel may reach another device: no remote copies, remote signals or barrier semaphores. Data moves between devices by JAX's collectives and lax.ppermute only.
A program may use at most 128 MiB of HBM per device.

v0:
```python
import functools

import jax
import jax.numpy as jnp
from jax import lax
from jax.experimental import pallas as pl
from jax.experimental.pallas import tpu as pltpu
from jax.sharding import PartitionSpec as P

CONV = 3
PAD = 16
gate_cap = 15.0
epsilon = 1e-06
far_below = -1e30
f32 = jnp.float32
bf16 = jnp.bfloat16


SMEM = pl.BlockSpec(memory_space=pltpu.SMEM)
VMEM = pl.BlockSpec(memory_space=pltpu.VMEM)
HBM = pl.BlockSpec(memory_space=pltpu.HBM)


def call(kernel, out, args, scratch=(), mib=16, loads=False, outside=()):
    specs = [SMEM if i == 0 else HBM if i in outside else VMEM for i in range(len(args))]
    args = [
        a
        if i == 0 or loads
        else pltpu.with_memory_space_constraint(a, pltpu.HBM if i in outside else pltpu.VMEM)
        for i, a in enumerate(args)
    ]
    many = isinstance(out[0][0], tuple)
    return pl.pallas_call(
        kernel,
        out_shape=tuple(jax.ShapeDtypeStruct(*o) for o in out)
        if many
        else jax.ShapeDtypeStruct(*out),
        in_specs=specs,
        out_specs=tuple(VMEM for _ in out) if many else VMEM,
        scratch_shapes=list(scratch),
        compiler_params=pltpu.CompilerParams(vmem_limit_bytes=mib * 2**20),
    )(*args)


def softcap(values):
    return gate_cap * jnp.tanh(values / gate_cap)


def log_gates(ig, fg):
    log_input = softcap(ig)
    capped = softcap(fg)
    log_forget = jnp.minimum(capped, 0.0) - jnp.log1p(jnp.exp(-jnp.abs(capped)))
    rows = ig.shape[1]
    lane = lax.broadcasted_iota(jnp.int32, (8, rows), 1)
    running = jnp.broadcast_to(log_forget, (8, rows))
    reach = 1
    while reach < rows:
        running = running + jnp.where(lane >= reach, pltpu.roll(running, reach, 1), 0.0)
        reach *= 2
    running = running[:1]
    return log_input, running


def column(row):
    return jnp.broadcast_to(row, (128, row.shape[1])).T[:, :1]


def store_state(ref, h, state):
    memory, normer, total, peak = state
    rows, hv = memory.shape
    side = jnp.concatenate(
        (
            normer,
            jnp.broadcast_to(total, (1, 128)),
            jnp.broadcast_to(peak, (1, hv - rows - 128)),
        ),
        axis=1,
    )
    high = side.astype(bf16).astype(f32)
    middle = (side - high).astype(bf16).astype(f32)
    low = (side - high - middle).astype(bf16).astype(f32)
    tail = jnp.concatenate((high, middle, low, jnp.zeros((13, hv), f32)), axis=0)
    ref[h, :rows, :] = memory.astype(bf16)
    ref[h, rows:, :] = tail.astype(bf16)


def load_state(ref, h):
    rows = ref.shape[1] - 16
    tail = ref[h, rows:, :].astype(f32)
    side = tail[0:1] + tail[1:2] + tail[2:3]
    return (
        ref[h, :rows, :].astype(f32),
        side[:, :rows],
        side[:, rows : rows + 1],
        side[:, rows + 128 : rows + 129],
    )


def combine(previous, following):
    prev_memory, prev_normer, prev_total, prev_peak = previous
    next_memory, next_normer, next_total, next_peak = following
    peak = jnp.maximum(next_total + prev_peak, next_peak)
    prev_scale = jnp.exp(next_total + prev_peak - peak)
    next_scale = jnp.exp(next_peak - peak)
    return (
        prev_scale * prev_memory + next_scale * next_memory,
        prev_scale * prev_normer + next_scale * next_normer,
        prev_total + next_total,
        peak,
    )


def summary_kernel(info, key, value, ig, fg, stay, go):
    heads = ig.shape[0]
    qk = key.shape[1] // heads
    hv = value.shape[1] // heads
    for h in range(heads):
        log_input, running = log_gates(ig[h : h + 1, :], fg[h : h + 1, :])
        total = running[:, -1:]
        lead = total - running + log_input
        peak = jnp.max(lead, axis=1, keepdims=True)
        weights = column(jnp.exp(lead - peak))
        weighted = key[:, h * qk : (h + 1) * qk].astype(f32) * weights
        memory = lax.dot_general(
            weighted.astype(bf16),
            value[:, h * hv : (h + 1) * hv],
            (((0,), (0,)), ((), ())),
            preferred_element_type=f32,
        )
        normer = jnp.sum(weighted, axis=0, keepdims=True)
        half = qk // 2
        halves = [
            (memory[:half], normer[:, :half], total, peak),
            (memory[half:], normer[:, half:], total, peak),
        ]
        for parity in range(2):

            @pl.when(info[1] == parity)
            def _():
                store_state(stay, h, halves[parity])
                store_state(go, h, halves[1 - parity])


def inner_kernel(info, query, key, value, ig, fg, numerator, side):
    heads = ig.shape[0]
    qk = key.shape[1] // heads
    hv = value.shape[1] // heads
    rows = key.shape[0]
    for h in range(heads):
        log_input, running = log_gates(ig[h : h + 1, :], fg[h : h + 1, :])
        running_column = column(running)
        causal = lax.broadcasted_iota(jnp.int32, (rows, rows), 0) >= lax.broadcasted_iota(
            jnp.int32, (rows, rows), 1
        )
        logs = jnp.where(causal, running_column - running + log_input, far_below)
        peak = jnp.max(logs, axis=1, keepdims=True)
        scores = lax.dot_general(
            query[:, h * qk : (h + 1) * qk] * bf16(qk**-0.5),
            key[:, h * qk : (h + 1) * qk],
            (((1,), (1,)), ((), ())),
            preferred_element_type=f32,
        ) * jnp.exp(logs - peak)
        numerator[:, h * hv : (h + 1) * hv] = jnp.dot(
            scores.astype(bf16), value[:, h * hv : (h + 1) * hv], preferred_element_type=f32
        )
        lane = lax.broadcasted_iota(jnp.int32, (rows, 128), 1)
        total = jnp.sum(scores, axis=1, keepdims=True)
        side[h] = jnp.where(lane == 0, total, jnp.where(lane == 1, peak, running_column))


def pair_kernel(info, mine, theirs, out):
    first = info[1] == 0
    for h in range(mine.shape[0]):
        own = load_state(mine, h)
        other = load_state(theirs, h)
        previous = tuple(jnp.where(first, a, b) for a, b in zip(own, other))
        following = tuple(jnp.where(first, b, a) for a, b in zip(own, other))
        store_state(out, h, combine(previous, following))


def combine_kernel(info, earlier, later, out):
    for h in range(earlier.shape[0]):
        store_state(out, h, combine(load_state(earlier, h), load_state(later, h)))


def entering_kernel(info, mine, theirs, *refs):
    states, keep, send = refs[:-2], refs[-2], refs[-1]
    first = info[1] == 0
    for h in range(mine.shape[0]):
        opening = tuple(
            jnp.where(first, a, b) for a, b in zip(load_state(mine, h), load_state(theirs, h))
        )
        before = None
        for ref in states:
            state = load_state(ref, h)
            before = state if before is None else combine(before, state)
        if before is None:
            before = tuple(jnp.zeros_like(a) for a in opening)
        after = combine(before, opening)
        store_state(keep, h, tuple(jnp.where(first, a, b) for a, b in zip(before, after)))
        store_state(send, h, tuple(jnp.where(first, b, a) for a, b in zip(before, after)))


def output_kernel(info, query, out_gate, numerator, side, mine, theirs, keep, send):
    heads = side.shape[0]
    qk = query.shape[1] // heads
    hv = out_gate.shape[1] // heads
    half = qk // 2
    blocks = 2 * keep.shape[0]
    step = keep.shape[1]
    for h in range(heads):
        own_half = pl.multiple_of(h * qk + info[1] * half, half)
        other_half = pl.multiple_of(h * qk + (1 - info[1]) * half, half)
        own_query = query[:, pl.ds(own_half, half)] * bf16(qk**-0.5)
        other_query = query[:, pl.ds(other_half, half)] * bf16(qk**-0.5)
        _, own_normer, _, before = load_state(mine, h)
        _, other_normer, _, _ = load_state(theirs, h)
        top = jnp.dot(own_query, mine[h, :half, :], preferred_element_type=f32) + jnp.dot(
            other_query, theirs[h, :half, :], preferred_element_type=f32
        )
        bottom = jnp.sum(
            own_query.astype(f32) * own_normer + other_query.astype(f32) * other_normer,
            axis=1,
            keepdims=True,
        )
        inner_total = side[h, :, 0:1]
        inner_peak = side[h, :, 1:2]
        carried = side[h, :, 2:3] + before
        peak = jnp.maximum(carried, inner_peak)
        outer = jnp.exp(carried - peak)
        inner = jnp.exp(inner_peak - peak)
        denominator = outer * bottom + inner * inner_total
        scale = 1.0 / jnp.maximum(jnp.abs(denominator), jnp.exp(-peak))
        cell = (outer * top + inner * numerator[:, h * hv : (h + 1) * hv]) * scale
        opened = cell * jax.nn.sigmoid(out_gate[:, h * hv : (h + 1) * hv].astype(f32))
        gated = opened.astype(bf16)
        for parity in range(2):

            @pl.when(info[3] == parity)
            def _():
                for j in range(blocks):
                    ref = keep if j % 2 == parity else send
                    ref[j // 2, :, h * hv : (h + 1) * hv] = gated[j * step : (j + 1) * step]


def project_kernel(shift, count, info, kept, got, own_weight, mate_weight, out):
    block = lax.rem(info[2] + shift, count)
    out[...] = (
        jnp.dot(kept[block], own_weight[...], preferred_element_type=f32)
        + jnp.dot(got[block], mate_weight[...], preferred_element_type=f32)
    ).astype(bf16)


def normalize(values, gains):
    return values * lax.rsqrt(jnp.mean(values * values, axis=-1, keepdims=True) + epsilon) * gains


def stream_kernel(info, residual, mix_gain, pre_gain, *refs):
    parts, stream_out, normed_out = refs[:-2], refs[-2], refs[-1]
    summed = parts[0][...].astype(f32)
    for part in parts[1:]:
        summed = summed + part[...].astype(f32)
    mixed = summed.astype(bf16).astype(f32)
    stream = (residual[...].astype(f32) + normalize(mixed, mix_gain[...])).astype(bf16)
    stream_out[...] = stream
    normed_out[...] = normalize(stream.astype(f32), pre_gain[...]).astype(bf16)


def chunk_of(info, k, e, nz, pair):
    z = lax.rem(info[0] - k + nz, nz)
    return z * 2 + jnp.bitwise_xor(info[1], e) if pair else z


def tiles_of(width):
    tile = 256 if width % 256 == 0 else width
    return [slice(t, t + tile) for t in range(0, width, tile)]


def times_weight(order, nz, pair, info, rows_all, blocks, span):
    rows = blocks[0].shape[0]
    product = None
    for (k, e), block in zip(order, blocks):
        start = pl.multiple_of(chunk_of(info, k, e, nz, pair) * rows, min(rows, 128))
        term = jnp.dot(
            rows_all[:, pl.ds(start, rows)], block[:, span], preferred_element_type=f32
        )
        product = term if product is None else product + term
    return product.astype(bf16)


def gate_kernel_(order, nz, pair, ny, info, *refs):
    halos = refs[:ny]
    pieces = refs[ny : 3 * ny]
    blocks = refs[3 * ny : 3 * ny + len(order)]
    out, rows_all, own, sem = refs[3 * ny + len(order) :]
    copy = pltpu.make_async_copy(blocks[0], own, sem)
    copy.start()
    blocks = (*blocks[1:], own)
    order = (*order[1:], order[0])
    halo = halos[0][...]
    for ref in halos[1:]:
        halo = halo + ref[...]
    rows_all[0:PAD, :] = halo
    step = pieces[0].shape[0]
    for i, piece in enumerate(pieces):
        d, other = i // 2, i % 2
        chip = lax.rem(info[2] - d + ny, ny)
        core = 1 - info[3] if other else info[3]
        start = pl.multiple_of(PAD + (chip * 2 + core) * step, 16)
        rows_all[pl.ds(start, step), :] = piece[...]
    copy.wait()
    for span in tiles_of(out.shape[1]):
        out[:, span] = times_weight(order, nz, pair, info, rows_all, blocks, span)


def up_kernel(order, nz, pair, info, gate_taps, value_taps, rows_all, gates, *refs):
    blocks = refs[: len(order)]
    keep, send, up = refs[len(order) :]
    ny, step, width = keep.shape
    total = 2 * ny * step
    up[0] = gates[...].astype(f32)
    for span in tiles_of(width):
        up[1, :, span] = times_weight(order, nz, pair, info, rows_all, blocks, span).astype(f32)
        summed = []
        for g, taps in enumerate((gate_taps, value_taps)):
            first = PAD - CONV + 1
            conv = taps[0:1, span] * up[g, first : first + total, span]
            for j in range(1, CONV):
                conv = conv + taps[j : j + 1, span] * up[g, first + j : first + j + total, span]
            summed.append(conv)
        hidden = (summed[0] / (1.0 + jnp.exp(-summed[0])) * summed[1]).astype(bf16)
        for parity in range(2):

            @pl.when(info[3] == parity)
            def _():
                for j in range(2 * ny):
                    ref = keep if j % 2 == parity else send
                    ref[j // 2, :, span] = hidden[j * step : (j + 1) * step]


def down_kernel(shift, info, keep, send, *refs):
    blocks, keep_out, send_out = refs[:-2], refs[-2], refs[-1]
    chip = lax.rem(info[2] + shift, keep.shape[0])
    step = keep.shape[1]
    both = jnp.concatenate((keep[chip], send[chip]), axis=0)
    start = 0
    for block in blocks:
        end = start + block.shape[0]
        product = lax.dot_general(
            both, block[...], (((1,), (1,)), ((), ())), preferred_element_type=f32
        ).astype(bf16)
        keep_out[:, start:end] = product[:step]
        send_out[:, start:end] = product[step:]
        start = end


def result_kernel(groups, rows, nz, pair, info, stream, post_gain, *refs):
    out, summed = refs[-2], refs[-1]
    count = (len(refs) - 2) // len(groups)
    for g, order in enumerate(groups):
        parts = refs[g * count : (g + 1) * count]
        total = parts[0][...].astype(f32)
        for part in parts[1:]:
            total = total + part[...].astype(f32)
        for i, (k, e) in enumerate(order):
            start = pl.multiple_of(chunk_of(info, k, e, nz, pair) * rows, min(rows, 128))
            summed[:, pl.ds(start, rows)] = total[:, i * rows : (i + 1) * rows]
    ffn = summed[...].astype(bf16).astype(f32)
    out[...] = (stream[...].astype(f32) + normalize(ffn, post_gain[...])).astype(bf16)


def is_small(n_sp, model):
    return n_sp <= 16 and model // n_sp % 128 == 0


def layer(
    query_rows,
    key_rows,
    value_rows,
    out_gate_pre,
    input_gate_pre,
    forget_gate_pre,
    residual,
    out_proj,
    mix_gain,
    pre_gain,
    gate_proj,
    value_proj,
    gate_kernel,
    value_kernel,
    down_proj,
    post_gain,
):
    n_sp = lax.axis_size("sp")
    n_tp = lax.axis_size("tp")
    nz = n_sp // 2
    ny = n_tp // 2
    rows, width = query_rows.shape[0], gate_proj.shape[1]
    heads = input_gate_pre.shape[0]
    qk = query_rows.shape[1] // heads
    hv = value_rows.shape[1] // heads
    model = residual.shape[1]
    step = rows // n_tp

    sp = lax.axis_index("sp")
    tp = lax.axis_index("tp")
    z, x = sp // 2, sp % 2
    lane = lax.iota(jnp.int32, 8)
    info = jnp.where(
        lane == 0, z, jnp.where(lane == 1, x, jnp.where(lane == 2, tp // 2, tp % 2))
    ).astype(jnp.int32)

    ring = [(i, (i + 2) % n_sp) for i in range(n_sp)]
    swap = [(i, i ^ 1) for i in range(n_sp)]

    mate = lambda a: lax.ppermute(a, "tp", [(i, i ^ 1) for i in range(n_tp)])
    chips = lambda a, d: lax.ppermute(a, "tp", [(i, (i + 2 * d) % n_tp) for i in range(n_tp)])

    def spread(block, name):
        found = {(0, 0): block}
        for k in range(nz):
            if k:
                found[k, 0] = lax.ppermute(found[k - 1, 0], "sp", ring)
            if name == "d" and k == 1:
                found[k, 1] = lax.ppermute(found[0, 1], "sp", ring)
            else:
                found[k, 1] = lax.ppermute(found[k, 0], "sp", swap)
        return found

    small = is_small(n_sp, model)
    if small:
        gates, values, downs = (
            spread(w, name)
            for w, name in ((gate_proj, "g"), (value_proj, "v"), (down_proj, "d"))
        )
        wide, paired = nz, True
    else:
        gates, values, downs = (
            {(0, 0): lax.all_gather(w, "sp", axis=0, tiled=True)}
            for w in (gate_proj, value_proj, down_proj)
        )
        wide, paired = 1, False
    order = tuple(gates)
    mate_proj = mate(out_proj)

    half_state = ((heads, qk // 2 + 16, hv), bf16)
    stay, go = call(
        summary_kernel,
        (half_state, half_state),
        (info, key_rows, value_rows, input_gate_pre, forget_gate_pre),
        loads=True,
    )
    partner = lax.ppermute(go, "sp", swap)
    total = call(pair_kernel, half_state, (info, stay, partner))
    states = []
    reach = 1
    while reach < nz:
        route = [(i, i + 2 * reach) for i in range(n_sp - 2 * reach)]
        states.insert(0, lax.ppermute(total, "sp", route))
        reach *= 2
        if reach < nz:
            total = call(combine_kernel, half_state, (info, states[0], total))
    before, across = call(entering_kernel, (half_state, half_state), (info, stay, partner, *states))
    across = lax.ppermute(across, "sp", swap)
    inner, side = call(
        inner_kernel,
        (((rows, heads * hv), f32), ((heads, rows, 128), f32)),
        (info, query_rows, key_rows, value_rows, input_gate_pre, forget_gate_pre),
    )
    kept, sent = call(
        output_kernel,
        (((ny, step, heads * hv), bf16), ((ny, step, heads * hv), bf16)),
        (info, query_rows, out_gate_pre, inner, side, before, across),
    )
    got = mate(sent)

    parts = []
    for d in [*range(1, ny), 0]:
        part = call(
            functools.partial(project_kernel, d, ny),
            ((step, model), bf16),
            (info, kept, got, out_proj, mate_proj),
        )
        parts.append(chips(part, d) if d else part)
    stream, normed = call(
        stream_kernel,
        (((step, model), bf16), ((step, model), bf16)),
        (info, residual, mix_gain[None], pre_gain[None], *parts),
    )

    pieces = []
    for d in range(ny):
        piece = chips(normed, d) if d else normed
        pieces += [piece, mate(piece)]
    last_rows = jnp.where(tp % 2 == 1, normed[step - PAD :], pieces[1][step - PAD :])
    halos = [
        lax.ppermute(
            last_rows,
            ("sp", "tp"),
            [
                (i * n_tp + n_tp - 2 + c, (i + 1) * n_tp + 2 * j + c)
                for i in range(n_sp - 1)
                for c in range(2)
            ],
        )
        for j in range(ny)
    ]

    up_gate, group_rows = call(
        functools.partial(gate_kernel_, order, wide, paired, ny),
        (((PAD + rows, width), bf16), ((PAD + rows, model), bf16)),
        (info, *halos, *pieces, *(gates[o] for o in order)),
        scratch=(pltpu.VMEM((model // len(order), width), bf16), pltpu.SemaphoreType.DMA),
        outside=(1 + ny + n_tp,),
    )
    hidden_keep, hidden_send = call(
        functools.partial(up_kernel, order, wide, paired),
        (((ny, step, width), bf16), ((ny, step, width), bf16)),
        (info, gate_kernel, value_kernel, group_rows, up_gate, *(values[o] for o in order)),
        scratch=(pltpu.VMEM((2, PAD + rows, width), f32),),
    )
    arrival = sorted(order, key=lambda o: o[0] + o[1] * {0: 1, 1: nz + 1}.get(o[0], nz - 1))
    cuts = [len(arrival) * i // 4 for i in (0, 2, 3, 4)]
    groups = [arrival[a:b] for a, b in zip(cuts, cuts[1:]) if b > a]
    rows_of = model // len(order)
    parts = [[] for _ in groups]
    for d in [*range(1, ny), 0]:
        for g, blocks in enumerate(groups):
            shape = ((step, rows_of * len(blocks)), bf16)
            mine, away = call(
                functools.partial(down_kernel, d),
                (shape, shape),
                (info, hidden_keep, hidden_send, *(downs[o] for o in blocks)),
            )
            theirs = mate(away)
            if d:
                both = (mine.astype(f32) + theirs.astype(f32)).astype(bf16)
                route = [(i, (i + 2 * d) % n_tp) for i in range(n_tp)]
                parts[g].append(lax.ppermute(both, "tp", route))
            else:
                parts[g] += [mine, theirs]
    return call(
        functools.partial(result_kernel, groups, rows_of, wide, paired),
        ((step, model), bf16),
        (info, stream, post_gain[None], *(p for group in parts for p in group)),
        scratch=(pltpu.VMEM((step, model), f32),),
    )


def solution(mesh):
    return jax.shard_map(
        layer,
        mesh=mesh,
        in_specs=(
            P("sp", "tp"),
            P("sp", "tp"),
            P("sp", "tp"),
            P("sp", "tp"),
            P("tp", "sp"),
            P("tp", "sp"),
            P(("sp", "tp"), None),
            P("tp", None),
            P(),
            P(),
            P("sp", "tp"),
            P("sp", "tp"),
            P(None, "tp"),
            P(None, "tp"),
            P("sp", "tp"),
            P(),
        ),
        out_specs=P(("sp", "tp"), None),
        check_vma=False,
    )
```

profile of v0, /device:TPU:0, one launch (start us, length us, event | category | flops | bytes accessed | tf_op | source)
XLA Modules:
  0.0 185.5 jit_solution(4672689458478159693)
XLA Ops:
  0.5 1.0 copy-done.1
  1.5 0.9 copy-done.4
  3.9 1.8 shard_map.155
  5.7 2.6 %collective-permute-start = (bf16[1,144,512]{2,1,0:T(8,128)(2,1)S(1)}, bf16[1,144,512]{2,1,0:T(8,128)(2,1)S(1)}, u32[]{:S(2)}, u32[]{:S(2)}) collective-permute-start(bf16[1,144,512]{2,1,0:T(8,128)(2,1)S(1)} %get-tuple-element.34), channel_id=1, source_target_pairs={{0,4},{4,0},{8,12},{12,8},{16,20},{20,16},{24,28},{28,24},{1,5},{5... | collective-permute-start | bytes 442376 | tf_op jit(solution)/shard_map/ppermute | solution.py:453
  8.3 4.5 %collective-permute-done.theirs = bf16[1,144,512]{2,1,0:T(8,128)(2,1)S(1)} collective-permute-done((bf16[1,144,512]{2,1,0:T(8,128)(2,1)S(1)}, bf16[1,144,512]{2,1,0:T(8,128)(2,1)S(1)}, u32[]{:S(2)}, u32[]{:S(2)}) %collective-permute-start) | collective-permute-done | bytes 147488 | tf_op jit(solution)/shard_map/ppermute | solution.py:453
  13.4 3.7 %collective-permute-start.1 = (bf16[1,144,512]{2,1,0:T(8,128)(2,1)S(1)}, bf16[1,144,512]{2,1,0:T(8,128)(2,1)S(1)}, u32[]{:S(2)}, u32[]{:S(2)}) collective-permute-start(bf16[1,144,512]{2,1,0:T(8,128)(2,1)S(1)} %shard_map.156.later), channel_id=1, source_target_pairs={{0,8},{4,12},{8,16},{12,20},{16,24},{20,28},{1,9},{5,13},{9,17},{1... | collective-permute-start | bytes 442376 | tf_op jit(solution)/shard_map/ppermute | solution.py:459
  17.2 2.8 %collective-permute-done.1.earlier.refs_1_ = bf16[1,144,512]{2,1,0:T(8,128)(2,1)S(1)} collective-permute-done((bf16[1,144,512]{2,1,0:T(8,128)(2,1)S(1)}, bf16[1,144,512]{2,1,0:T(8,128)(2,1)S(1)}, u32[]{:S(2)}, u32[]{:S(2)}) %collective-permute-start.1) | collective-permute-done | bytes 147488 | tf_op jit(solution)/shard_map/ppermute | solution.py:459
  20.7 5.5 %collective-permute-start.2 = (bf16[1,144,512]{2,1,0:T(8,128)(2,1)S(1)}, bf16[1,144,512]{2,1,0:T(8,128)(2,1)S(1)}, u32[]{:S(2)}, u32[]{:S(2)}) collective-permute-start(bf16[1,144,512]{2,1,0:T(8,128)(2,1)S(1)} %shard_map.157), channel_id=1, source_target_pairs={{0,16},{4,20},{8,24},{12,28},{1,17},{5,21},{9,25},{13,29},{2,18},{... | collective-permute-start | bytes 442376 | tf_op jit(solution)/shard_map/ppermute | solution.py:459
  26.3 2.7 %collective-permute-done.2.refs_0_ = bf16[1,144,512]{2,1,0:T(8,128)(2,1)S(1)} collective-permute-done((bf16[1,144,512]{2,1,0:T(8,128)(2,1)S(1)}, bf16[1,144,512]{2,1,0:T(8,128)(2,1)S(1)}, u32[]{:S(2)}, u32[]{:S(2)}) %collective-permute-start.2) | collective-permute-done | bytes 147488 | tf_op jit(solution)/shard_map/ppermute | solution.py:459
  28.9 0.8 shard_map.158
  29.7 1.6 collective-permute-start.3
  31.3 1.9 %shard_map.154 = (f32[512,512]{1,0:T(8,128)S(1)}, f32[1,512,128]{2,1,0:T(8,128)S(1)}) custom-call(s32[8]{0:T(128)S(1)} %compare_select_fusion.2.info, bf16[512,256]{1,0:T(8,128)(2,1)S(1)} %copy-done.6, bf16[512,256]{1,0:T(8,128)(2,1)S(1)} %copy-done.5, bf16[512,512]{1,0:T(8,128)(2,1)S(1)} %copy-done.2, f32[1,512]{1,0:T(1,128)S(1)} %copy-done.33, ...), custom_call_target="tpu_custom_call" | custom-call | tf_op jit(solution)/shard_map/pallas_call | solution.py:33
  33.2 1.8 collective-permute-done.3.theirs
  34.9 1.4 shard_map.159
  36.5 1.5 collective-permute-start.12
  38.0 1.3 shard_map.160
  39.4 1.6 collective-permute-start.6
  40.9 3.9 %collective-permute-start.13 = (bf16[256,768]{1,0:T(8,128)(2,1)S(1)}, bf16[256,768]{1,0:T(8,128)(2,1)S(1)}, u32[]{:S(2)}, u32[]{:S(2)}) collective-permute-start(bf16[256,768]{1,0:T(8,128)(2,1)S(1)} %copy-done.36), channel_id=1, source_target_pairs={{0,8},{4,12},{8,16},{12,20},{16,24},{20,28},{24,0},{28,4},{1,9},{5... | collective-permute-start | bytes 1179656 | tf_op jit(solution)/shard_map/ppermute | solution.py:423
  44.9 1.4 collective-permute-start.19
  46.4 2.1 %collective-permute-done.12.refs_7_ = bf16[256,768]{1,0:T(8,128)(2,1)S(1)} collective-permute-done((bf16[256,768]{1,0:T(8,128)(2,1)S(1)}, bf16[256,768]{1,0:T(8,128)(2,1)S(1)}, u32[]{:S(2)}, u32[]{:S(2)}) %collective-permute-start.12) | collective-permute-done | bytes 393248 | tf_op jit(solution)/shard_map/ppermute | solution.py:427
  48.5 1.5 collective-permute-start.26
  50.0 7.7 %collective-permute-done.13.refs_8_ = bf16[256,768]{1,0:T(8,128)(2,1)S(1)} collective-permute-done((bf16[256,768]{1,0:T(8,128)(2,1)S(1)}, bf16[256,768]{1,0:T(8,128)(2,1)S(1)}, u32[]{:S(2)}, u32[]{:S(2)}) %collective-permute-start.13) | collective-permute-done | bytes 393248 | tf_op jit(solution)/shard_map/ppermute | solution.py:423
  57.7 1.5 collective-permute-start.14
  59.2 7.1 %collective-permute-done.20.refs_2_ = bf16[256,768]{1,0:T(8,128)(2,1)} collective-permute-done((bf16[256,768]{1,0:T(8,128)(2,1)S(1)}, bf16[256,768]{1,0:T(8,128)(2,1)}, u32[]{:S(2)}, u32[]{:S(2)}) %collective-permute-start.20) | collective-permute-done | bytes 393248 | tf_op jit(solution)/shard_map/ppermute | solution.py:423
  66.2 1.4 collective-permute-start.21
  67.6 1.3 shard_map.161.refs_1_
  69.0 1.1 shard_map.162
  70.1 0.8 copy-done.13
  70.9 3.7 %collective-permute-done.27.refs_2_ = bf16[256,768]{1,0:T(8,128)(2,1)S(1)} collective-permute-done((bf16[256,768]{1,0:T(8,128)(2,1)S(1)}, bf16[256,768]{1,0:T(8,128)(2,1)S(1)}, u32[]{:S(2)}, u32[]{:S(2)}) %collective-permute-start.27) | collective-permute-done | bytes 393248 | tf_op jit(solution)/shard_map/ppermute | solution.py:423
  75.8 2.7 %collective-permute-start.22 = (bf16[256,768]{1,0:T(8,128)(2,1)}, bf16[256,768]{1,0:T(8,128)(2,1)}, u32[]{:S(2)}, u32[]{:S(2)}) collective-permute-start(bf16[256,768]{1,0:T(8,128)(2,1)} %collective-permute-done.20.refs_2_), channel_id=1, source_target_pairs={{0,8},{4,12},{8,16},{12,20},{16,24},{20,28},{24,0},{28,4},{1,9},{5... | collective-permute-start | bytes 1179656 | tf_op jit(solution)/shard_map/ppermute | solution.py:423
  78.5 4.4 %collective-permute-done.15.refs_10_ = bf16[256,768]{1,0:T(8,128)(2,1)} collective-permute-done((bf16[256,768]{1,0:T(8,128)(2,1)S(1)}, bf16[256,768]{1,0:T(8,128)(2,1)}, u32[]{:S(2)}, u32[]{:S(2)}) %collective-permute-start.15) | collective-permute-done | bytes 393248 | tf_op jit(solution)/shard_map/ppermute | solution.py:423
  82.9 0.8 copy-done.19
  83.6 2.7 %collective-permute-start.17 = (bf16[256,768]{1,0:T(8,128)(2,1)}, bf16[256,768]{1,0:T(8,128)(2,1)}, u32[]{:S(2)}, u32[]{:S(2)}) collective-permute-start(bf16[256,768]{1,0:T(8,128)(2,1)} %collective-permute-done.15.refs_10_), channel_id=1, source_target_pairs={{0,8},{4,12},{8,16},{12,20},{16,24},{20,28},{24,0},{28,4},{1,9},{5... | collective-permute-start | bytes 1179656 | tf_op jit(solution)/shard_map/ppermute | solution.py:423
  86.4 5.2 %collective-permute-done.22.refs_4_ = bf16[256,768]{1,0:T(8,128)(2,1)} collective-permute-done((bf16[256,768]{1,0:T(8,128)(2,1)}, bf16[256,768]{1,0:T(8,128)(2,1)}, u32[]{:S(2)}, u32[]{:S(2)}) %collective-permute-start.22) | collective-permute-done | bytes 393248 | tf_op jit(solution)/shard_map/ppermute | solution.py:423
  91.6 1.5 collective-permute-start.16
  93.0 6.8 %collective-permute-done.28.refs_3_ = bf16[256,768]{1,0:T(8,128)(2,1)S(1)} collective-permute-done((bf16[256,768]{1,0:T(8,128)(2,1)S(1)}, bf16[256,768]{1,0:T(8,128)(2,1)S(1)}, u32[]{:S(2)}, u32[]{:S(2)}) %collective-permute-start.28) | collective-permute-done | bytes 393248 | tf_op jit(solution)/shard_map/ppermute | solution.py:423
  99.9 8.5 %collective-permute-done.17.refs_12_ = bf16[256,768]{1,0:T(8,128)(2,1)} collective-permute-done((bf16[256,768]{1,0:T(8,128)(2,1)}, bf16[256,768]{1,0:T(8,128)(2,1)}, u32[]{:S(2)}, u32[]{:S(2)}) %collective-permute-start.17) | collective-permute-done | bytes 393248 | tf_op jit(solution)/shard_map/ppermute | solution.py:423
  108.4 1.5 collective-permute-start.18
  110.0 0.8 copy-done.7
  110.7 0.8 copy-done.9
  112.1 4.6 %collective-permute-done.24.refs_6_ = bf16[256,768]{1,0:T(8,128)(2,1)S(1)} collective-permute-done((bf16[256,768]{1,0:T(8,128)(2,1)}, bf16[256,768]{1,0:T(8,128)(2,1)S(1)}, u32[]{:S(2)}, u32[]{:S(2)}) %collective-permute-start.24) | collective-permute-done | bytes 393248 | tf_op jit(solution)/shard_map/ppermute | solution.py:423
  116.7 1.5 collective-permute-start.25
  118.2 6.0 %collective-permute-done.32.refs_0_ = bf16[256,768]{1,0:T(8,128)(2,1)S(1)} collective-permute-done((bf16[256,768]{1,0:T(8,128)(2,1)S(1)}, bf16[256,768]{1,0:T(8,128)(2,1)S(1)}, u32[]{:S(2)}, u32[]{:S(2)}) %collective-permute-start.32) | collective-permute-done | bytes 393248 | tf_op jit(solution)/shard_map/ppermute | solution.py:423
  124.9 2.1 %collective-permute-start.33 = (bf16[256,768]{1,0:T(8,128)(2,1)S(1)}, bf16[256,768]{1,0:T(8,128)(2,1)S(1)}, u32[]{:S(2)}, u32[]{:S(2)}) collective-permute-start(bf16[256,768]{1,0:T(8,128)(2,1)S(1)} %collective-permute-done.28.refs_3_), channel_id=1, source_target_pairs={{0,4},{4,0},{8,12},{12,8},{16,20},{20,16},{24,28},{28,24},{1,5},{5... | collective-permute-start | bytes 1179656 | tf_op jit(solution)/shard_map/ppermute | solution.py:427
  127.7 4.2 %collective-permute-start.37 = (bf16[256,768]{1,0:T(8,128)(2,1)S(1)}, bf16[256,768]{1,0:T(8,128)(2,1)S(1)}, u32[]{:S(2)}, u32[]{:S(2)}) collective-permute-start(bf16[256,768]{1,0:T(8,128)(2,1)S(1)} %collective-permute-done.26.refs_1_), channel_id=1, source_target_pairs={{0,8},{4,12},{8,16},{12,20},{16,24},{20,28},{24,0},{28,4},{1,9},{5... | collective-permute-start | bytes 1179656 | tf_op jit(solution)/shard_map/ppermute | solution.py:425
  132.0 9.0 %collective-permute-start.38 = (bf16[256,768]{1,0:T(8,128)(2,1)S(1)}, bf16[256,768]{1,0:T(8,128)(2,1)S(1)}, u32[]{:S(2)}, u32[]{:S(2)}) collective-permute-start(bf16[256,768]{1,0:T(8,128)(2,1)S(1)} %collective-permute-done.32.refs_0_), channel_id=1, source_target_pairs={{0,4},{4,0},{8,12},{12,8},{16,20},{20,16},{24,28},{28,24},{1,5},{5... | collective-permute-start | bytes 1179656 | tf_op jit(solution)/shard_map/ppermute | solution.py:427
  141.0 1.0 copy-done.8
  142.0 1.0 copy-done.10
  143.1 1.0 copy-done.22
  144.1 1.0 copy-done.24
  145.1 1.0 copy-done.26
  146.1 4.3 %shard_map.163 = (bf16[528,768]{1,0:T(8,128)(2,1)S(1)}, bf16[528,2048]{1,0:T(8,128)(2,1)S(1)}) custom-call(s32[8]{0:T(128)S(1)} %compare_select_fusion.2.info, bf16[16,2048]{1,0:T(8,128)(2,1)S(1)} %collective-permute-done.8.refs_0_, bf16[16,2048]{1,0:T(8,128)(2,1)S(1)} %collective-permute-done.9.refs_1_, bf16[128,2048]{1,0:T(8,128)(2,1)S(1)} %copy-done.8, ...), custom_call_target="tpu_custom_call" | custom-call | tf_op jit(solution)/shard_map/pallas_call | solution.py:33
  150.4 5.7 %shard_map.164 = (bf16[2,128,768]{2,1,0:T(8,128)(2,1)S(1)}, bf16[2,128,768]{2,1,0:T(8,128)(2,1)S(1)}) custom-call(s32[8]{0:T(128)S(1)} %compare_select_fusion.2.info, f32[3,768]{1,0:T(4,128)S(1)} %copy-done.27, f32[3,768]{1,0:T(4,128)S(1)} %copy-done.28, bf16[528,2048]{1,0:T(8,128)(2,1)S(1)} %get-tuple-element.41.rows_all, ...), custom_call_target="tpu_custom_call" | custom-call | tf_op jit(solution)/shard_map/pallas_call | solution.py:33
  156.1 0.9 shard_map.167
  157.1 1.1 shard_map.165
  158.9 1.1 shard_map.166
  160.1 0.9 shard_map.168
  161.6 0.9 shard_map.169
  162.7 0.9 shard_map.170
  164.2 7.2 %collective-permute-start.35 = (bf16[128,512]{1,0:T(8,128)(2,1)S(1)}, bf16[128,512]{1,0:T(8,128)(2,1)S(1)}, u32[]{:S(2)}, u32[]{:S(2)}) collective-permute-start(bf16[128,512]{1,0:T(8,128)(2,1)S(1)} %add_convert_fusion.2), channel_id=1, source_target_pairs={{0,2},{1,3},{2,0},{3,1},{4,6},{5,7},{6,4},{7,5},{8,10},{9,11},{10,... | collective-permute-start | bytes 393224 | tf_op jit(solution)/shard_map/ppermute | solution.py:539
  171.7 2.1 %collective-permute-start.40 = (bf16[128,512]{1,0:T(8,128)(2,1)S(1)}, bf16[128,512]{1,0:T(8,128)(2,1)S(1)}, u32[]{:S(2)}, u32[]{:S(2)}) collective-permute-start(bf16[128,512]{1,0:T(8,128)(2,1)S(1)} %add_convert_fusion.1), channel_id=1, source_target_pairs={{0,2},{1,3},{2,0},{3,1},{4,6},{5,7},{6,4},{7,5},{8,10},{9,11},{10,... | collective-permute-start | bytes 393224 | tf_op jit(solution)/shard_map/ppermute | solution.py:539
  173.7 2.1 %collective-permute-done.35.refs_3_ = bf16[128,512]{1,0:T(8,128)(2,1)S(1)} collective-permute-done((bf16[128,512]{1,0:T(8,128)(2,1)S(1)}, bf16[128,512]{1,0:T(8,128)(2,1)S(1)}, u32[]{:S(2)}, u32[]{:S(2)}) %collective-permute-start.35) | collective-permute-done | bytes 131104 | tf_op jit(solution)/shard_map/ppermute | solution.py:539
  175.8 7.8 %collective-permute-done.40.refs_6_ = bf16[128,512]{1,0:T(8,128)(2,1)S(1)} collective-permute-done((bf16[128,512]{1,0:T(8,128)(2,1)S(1)}, bf16[128,512]{1,0:T(8,128)(2,1)S(1)}, u32[]{:S(2)}, u32[]{:S(2)}) %collective-permute-start.40) | collective-permute-done | bytes 131104 | tf_op jit(solution)/shard_map/ppermute | solution.py:539
  183.6 2.0 %shard_map.171 = bf16[128,2048]{1,0:T(8,128)(2,1)} custom-call(s32[8]{0:T(128)S(1)} %compare_select_fusion.2.info, bf16[128,2048]{1,0:T(8,128)(2,1)S(1)} %copy-done.14, f32[1,2048]{1,0:T(1,128)S(1)} %bitcast.5, bf16[128,1024]{1,0:T(8,128)(2,1)S(1)} %collective-permute-done.30.refs_0_, bf16[128,1024]{1,0:T(8,128)(2,1)S(1)} %get-tuple-element.47.refs_1_, ...), custom_call_target="tpu_custom_call" | custom-call | tf_op jit(solution)/shard_map/pallas_call | solution.py:33
  (117 shorter events, 8.8 us)
Async XLA Ops:
  0.0 31.3 %copy-start.33 = (f32[1,512]{1,0:T(1,128)S(1)}, f32[1,512]{1,0:T(1,128)}, u32[]{:S(2)}) copy-start(f32[1,512]{1,0:T(1,128)} %ig.3) | copy-start | bytes 6148
  0.0 31.3 %copy-start.35 = (f32[1,512]{1,0:T(1,128)S(1)}, f32[1,512]{1,0:T(1,128)}, u32[]{:S(2)}) copy-start(f32[1,512]{1,0:T(1,128)} %fg.3) | copy-start | bytes 6148
  0.0 38.0 %collective-permute-start.5 = (bf16[512,2048]{1,0:T(8,128)(2,1)}, bf16[512,2048]{1,0:T(8,128)(2,1)S(1)}, u32[]{:S(2)}, u32[]{:S(2)}) collective-permute-start(bf16[512,2048]{1,0:T(8,128)(2,1)} %own_weight.3), channel_id=1, source_target_pairs={{0,1},{1,0},{2,3},{3,2},{4,5},{5,4},{6,7},{7,6},{8,9},{9,8},{10,11... | collective-permute-start | bytes 6291464 | tf_op jit(solution)/shard_map/ppermute | solution.py:416
  3.9 27.4 %copy-start.2 = (bf16[512,512]{1,0:T(8,128)(2,1)S(1)}, bf16[512,512]{1,0:T(8,128)(2,1)}, u32[]{:S(2)}) copy-start(bf16[512,512]{1,0:T(8,128)(2,1)} %value.3) | copy-start | bytes 1572868
  3.9 27.4 %copy-start.5 = (bf16[512,256]{1,0:T(8,128)(2,1)S(1)}, bf16[512,256]{1,0:T(8,128)(2,1)}, u32[]{:S(2)}) copy-start(bf16[512,256]{1,0:T(8,128)(2,1)} %key.3) | copy-start | bytes 786436
  3.9 27.4 %copy-start.6 = (bf16[512,256]{1,0:T(8,128)(2,1)S(1)}, bf16[512,256]{1,0:T(8,128)(2,1)}, u32[]{:S(2)}) copy-start(bf16[512,256]{1,0:T(8,128)(2,1)} %query.3) | copy-start | bytes 786436
  3.9 31.1 %copy-start.12 = (bf16[512,512]{1,0:T(8,128)(2,1)S(1)}, bf16[512,512]{1,0:T(8,128)(2,1)}, u32[]{:S(2)}) copy-start(bf16[512,512]{1,0:T(8,128)(2,1)} %out_gate.1) | copy-start | bytes 1572868
  5.7 7.1 %collective-permute-start = (bf16[1,144,512]{2,1,0:T(8,128)(2,1)S(1)}, bf16[1,144,512]{2,1,0:T(8,128)(2,1)S(1)}, u32[]{:S(2)}, u32[]{:S(2)}) collective-permute-start(bf16[1,144,512]{2,1,0:T(8,128)(2,1)S(1)} %get-tuple-element.34), channel_id=1, source_target_pairs={{0,4},{4,0},{8,12},{12,8},{16,20},{20,16},{24,28},{28,24},{1,5},{5... | collective-permute-start | bytes 442376 | tf_op jit(solution)/shard_map/ppermute | solution.py:453
  13.4 6.6 %collective-permute-start.1 = (bf16[1,144,512]{2,1,0:T(8,128)(2,1)S(1)}, bf16[1,144,512]{2,1,0:T(8,128)(2,1)S(1)}, u32[]{:S(2)}, u32[]{:S(2)}) collective-permute-start(bf16[1,144,512]{2,1,0:T(8,128)(2,1)S(1)} %shard_map.156.later), channel_id=1, source_target_pairs={{0,8},{4,12},{8,16},{12,20},{16,24},{20,28},{1,9},{5,13},{9,17},{1... | collective-permute-start | bytes 442376 | tf_op jit(solution)/shard_map/ppermute | solution.py:459
  20.7 15.8 %copy-start.36 = (bf16[256,768]{1,0:T(8,128)(2,1)S(1)}, bf16[256,768]{1,0:T(8,128)(2,1)}, u32[]{:S(2)}) copy-start(bf16[256,768]{1,0:T(8,128)(2,1)} %refs_6_.1) | copy-start | bytes 1179652
  20.7 17.3 %copy-start = (bf16[512,2048]{1,0:T(8,128)(2,1)S(1)}, bf16[512,2048]{1,0:T(8,128)(2,1)}, u32[]{:S(2)}) copy-start(bf16[512,2048]{1,0:T(8,128)(2,1)} %own_weight.3) | copy-start | bytes 6291460
  20.7 8.2 %collective-permute-start.2 = (bf16[1,144,512]{2,1,0:T(8,128)(2,1)S(1)}, bf16[1,144,512]{2,1,0:T(8,128)(2,1)S(1)}, u32[]{:S(2)}, u32[]{:S(2)}) collective-permute-start(bf16[1,144,512]{2,1,0:T(8,128)(2,1)S(1)} %shard_map.157), channel_id=1, source_target_pairs={{0,16},{4,20},{8,24},{12,28},{1,17},{5,21},{9,25},{13,29},{2,18},{... | collective-permute-start | bytes 442376 | tf_op jit(solution)/shard_map/ppermute | solution.py:459
  29.7 5.2 %collective-permute-start.3 = (bf16[1,144,512]{2,1,0:T(8,128)(2,1)S(1)}, bf16[1,144,512]{2,1,0:T(8,128)(2,1)S(1)}, u32[]{:S(2)}, u32[]{:S(2)}) collective-permute-start(bf16[1,144,512]{2,1,0:T(8,128)(2,1)S(1)} %get-tuple-element.36), channel_id=1, source_target_pairs={{0,4},{4,0},{8,12},{12,8},{16,20},{20,16},{24,28},{28,24},{1,5},{5... | collective-permute-start | bytes 442376 | tf_op jit(solution)/shard_map/ppermute | solution.py:464
  36.4 1.6 collective-permute-start.4
  36.5 12.1 %collective-permute-start.12 = (bf16[256,768]{1,0:T(8,128)(2,1)S(1)}, bf16[256,768]{1,0:T(8,128)(2,1)S(1)}, u32[]{:S(2)}, u32[]{:S(2)}) collective-permute-start(bf16[256,768]{1,0:T(8,128)(2,1)S(1)} %copy-done.36), channel_id=1, source_target_pairs={{0,4},{4,0},{8,12},{12,8},{16,20},{20,16},{24,28},{28,24},{1,5},{5... | collective-permute-start | bytes 1179656 | tf_op jit(solution)/shard_map/ppermute | solution.py:427
  38.0 6.9 %copy-start.15 = (bf16[256,768]{1,0:T(8,128)(2,1)S(1)}, bf16[256,768]{1,0:T(8,128)(2,1)}, u32[]{:S(2)}) copy-start(bf16[256,768]{1,0:T(8,128)(2,1)} %refs_0_.3) | copy-start | bytes 1179652
  38.0 10.5 %copy-start.3 = (bf16[256,768]{1,0:T(8,128)(2,1)S(1)}, bf16[256,768]{1,0:T(8,128)(2,1)}, u32[]{:S(2)}) copy-start(bf16[256,768]{1,0:T(8,128)(2,1)} %refs_0_.5) | copy-start | bytes 1179652
  39.3 29.6 %copy-start.11 = (bf16[128,2048]{1,0:T(8,128)(2,1)S(1)}, bf16[128,2048]{1,0:T(8,128)(2,1)}, u32[]{:S(2)}) copy-start(bf16[128,2048]{1,0:T(8,128)(2,1)} %residual.1) | copy-start | bytes 1572868
  39.3 29.6 %copy-start.29 = (f32[2048]{0:T(1024)S(1)}, f32[2048]{0:T(1024)}, u32[]{:S(2)}) copy-start(f32[2048]{0:T(1024)} %param.24) | copy-start | bytes 24580
  39.4 29.6 %copy-start.30 = (f32[2048]{0:T(1024)S(1)}, f32[2048]{0:T(1024)}, u32[]{:S(2)}) copy-start(f32[2048]{0:T(1024)} %param.25) | copy-start | bytes 24580
  39.4 26.9 %collective-permute-start.6 = (bf16[128,2048]{1,0:T(8,128)(2,1)S(1)}, bf16[128,2048]{1,0:T(8,128)(2,1)S(1)}, u32[]{:S(2)}, u32[]{:S(2)}) collective-permute-start(bf16[128,2048]{1,0:T(8,128)(2,1)S(1)} %shard_map.160), channel_id=1, source_target_pairs={{0,2},{1,3},{2,0},{3,1},{4,6},{5,7},{6,4},{7,5},{8,10},{9,11},{10,... | collective-permute-start | bytes 1572872 | tf_op jit(solution)/shard_map/ppermute | solution.py:417
  40.9 16.8 %collective-permute-start.13 = (bf16[256,768]{1,0:T(8,128)(2,1)S(1)}, bf16[256,768]{1,0:T(8,128)(2,1)S(1)}, u32[]{:S(2)}, u32[]{:S(2)}) collective-permute-start(bf16[256,768]{1,0:T(8,128)(2,1)S(1)} %copy-done.36), channel_id=1, source_target_pairs={{0,8},{4,12},{8,16},{12,20},{16,24},{20,28},{24,0},{28,4},{1,9},{5... | collective-permute-start | bytes 1179656 | tf_op jit(solution)/shard_map/ppermute | solution.py:423
  44.9 12.8 %collective-permute-start.19 = (bf16[256,768]{1,0:T(8,128)(2,1)S(1)}, bf16[256,768]{1,0:T(8,128)(2,1)S(1)}, u32[]{:S(2)}, u32[]{:S(2)}) collective-permute-start(bf16[256,768]{1,0:T(8,128)(2,1)S(1)} %copy-done.15), channel_id=1, source_target_pairs={{0,4},{4,0},{8,12},{12,8},{16,20},{20,16},{24,28},{28,24},{1,5},{5... | collective-permute-start | bytes 1179656 | tf_op jit(solution)/shard_map/ppermute | solution.py:427
  46.3 19.9 %collective-permute-start.20 = (bf16[256,768]{1,0:T(8,128)(2,1)S(1)}, bf16[256,768]{1,0:T(8,128)(2,1)}, u32[]{:S(2)}, u32[]{:S(2)}) collective-permute-start(bf16[256,768]{1,0:T(8,128)(2,1)S(1)} %copy-done.15), channel_id=1, source_target_pairs={{0,8},{4,12},{8,16},{12,20},{16,24},{20,28},{24,0},{28,4},{1,9},{5... | collective-permute-start | bytes 1179656 | tf_op jit(solution)/shard_map/ppermute | solution.py:423
  48.5 20.4 %copy-start.21 = (bf16[256,768]{1,0:T(8,128)(2,1)}, bf16[256,768]{1,0:T(8,128)(2,1)S(1)}, u32[]{:S(2)}) copy-start(bf16[256,768]{1,0:T(8,128)(2,1)S(1)} %collective-permute-done.12.refs_7_) | copy-start | bytes 1179652
  48.5 22.4 %collective-permute-start.26 = (bf16[256,768]{1,0:T(8,128)(2,1)S(1)}, bf16[256,768]{1,0:T(8,128)(2,1)S(1)}, u32[]{:S(2)}, u32[]{:S(2)}) collective-permute-start(bf16[256,768]{1,0:T(8,128)(2,1)S(1)} %copy-done.3), channel_id=1, source_target_pairs={{0,4},{4,0},{8,12},{12,8},{16,20},{20,16},{24,28},{28,24},{1,5},{5... | collective-permute-start | bytes 1179656 | tf_op jit(solution)/shard_map/ppermute | solution.py:427
  57.7 11.2 %copy-start.23 = (bf16[256,768]{1,0:T(8,128)(2,1)}, bf16[256,768]{1,0:T(8,128)(2,1)S(1)}, u32[]{:S(2)}) copy-start(bf16[256,768]{1,0:T(8,128)(2,1)S(1)} %collective-permute-done.13.refs_8_) | copy-start | bytes 1179652
  57.7 16.9 %collective-permute-start.27 = (bf16[256,768]{1,0:T(8,128)(2,1)S(1)}, bf16[256,768]{1,0:T(8,128)(2,1)S(1)}, u32[]{:S(2)}, u32[]{:S(2)}) collective-permute-start(bf16[256,768]{1,0:T(8,128)(2,1)S(1)} %copy-done.3), channel_id=1, source_target_pairs={{0,8},{4,12},{8,16},{12,20},{16,24},{20,28},{24,0},{28,4},{1,9},{5... | collective-permute-start | bytes 1179656 | tf_op jit(solution)/shard_map/ppermute | solution.py:423
  57.7 11.2 %copy-start.17 = (bf16[256,768]{1,0:T(8,128)(2,1)}, bf16[256,768]{1,0:T(8,128)(2,1)S(1)}, u32[]{:S(2)}) copy-start(bf16[256,768]{1,0:T(8,128)(2,1)S(1)} %collective-permute-done.19.refs_1_) | copy-start | bytes 1179652
  57.7 17.3 %collective-permute-start.14 = (bf16[256,768]{1,0:T(8,128)(2,1)S(1)}, bf16[256,768]{1,0:T(8,128)(2,1)S(1)}, u32[]{:S(2)}, u32[]{:S(2)}) collective-permute-start(bf16[256,768]{1,0:T(8,128)(2,1)S(1)} %collective-permute-done.13.refs_8_), channel_id=1, source_target_pairs={{0,4},{4,0},{8,12},{12,8},{16,20},{20,16},{24,28},{28,24},{1,5},{5... | collective-permute-start | bytes 1179656 | tf_op jit(solution)/shard_map/ppermute | solution.py:427
  66.2 16.6 %collective-permute-start.15 = (bf16[256,768]{1,0:T(8,128)(2,1)S(1)}, bf16[256,768]{1,0:T(8,128)(2,1)}, u32[]{:S(2)}, u32[]{:S(2)}) collective-permute-start(bf16[256,768]{1,0:T(8,128)(2,1)S(1)} %collective-permute-done.13.refs_8_), channel_id=1, source_target_pairs={{0,8},{4,12},{8,16},{12,20},{16,24},{20,28},{24,0},{28,4},{1,9},{5... | collective-permute-start | bytes 1179656 | tf_op jit(solution)/shard_map/ppermute | solution.py:423
  66.2 16.6 %collective-permute-start.21 = (bf16[256,768]{1,0:T(8,128)(2,1)}, bf16[256,768]{1,0:T(8,128)(2,1)S(1)}, u32[]{:S(2)}, u32[]{:S(2)}) collective-permute-start(bf16[256,768]{1,0:T(8,128)(2,1)} %collective-permute-done.20.refs_2_), channel_id=1, source_target_pairs={{0,4},{4,0},{8,12},{12,8},{16,20},{20,16},{24,28},{28,24},{1,5},{5... | collective-permute-start | bytes 1179656 | tf_op jit(solution)/shard_map/ppermute | solution.py:427
  70.9 37.5 %collective-permute-start.7 = (bf16[128,2048]{1,0:T(8,128)(2,1)S(1)}, bf16[128,2048]{1,0:T(8,128)(2,1)S(1)}, u32[]{:S(2)}, u32[]{:S(2)}) collective-permute-start(bf16[128,2048]{1,0:T(8,128)(2,1)S(1)} %get-tuple-element.40.refs_2_), channel_id=1, source_target_pairs={{0,1},{1,0},{2,3},{3,2},{4,5},{5,4},{6,7},{7,6},{8,9},{9,8},{10,11... | collective-permute-start | bytes 1572872 | tf_op jit(solution)/shard_map/ppermute | solution.py:416
  74.6 35.4 %collective-permute-start.10 = (bf16[128,2048]{1,0:T(8,128)(2,1)S(1)}, bf16[128,2048]{1,0:T(8,128)(2,1)}, u32[]{:S(2)}, u32[]{:S(2)}) collective-permute-start(bf16[128,2048]{1,0:T(8,128)(2,1)S(1)} %get-tuple-element.40.refs_2_), channel_id=1, source_target_pairs={{0,2},{1,3},{2,0},{3,1},{4,6},{5,7},{6,4},{7,5},{8,10},{9,11},{10,... | collective-permute-start | bytes 1572872 | tf_op jit(solution)/shard_map/ppermute | solution.py:417
  75.8 15.8 %collective-permute-start.22 = (bf16[256,768]{1,0:T(8,128)(2,1)}, bf16[256,768]{1,0:T(8,128)(2,1)}, u32[]{:S(2)}, u32[]{:S(2)}) collective-permute-start(bf16[256,768]{1,0:T(8,128)(2,1)} %collective-permute-done.20.refs_2_), channel_id=1, source_target_pairs={{0,8},{4,12},{8,16},{12,20},{16,24},{20,28},{24,0},{28,4},{1,9},{5... | collective-permute-start | bytes 1179656 | tf_op jit(solution)/shard_map/ppermute | solution.py:423
  82.9 17.0 %collective-permute-start.28 = (bf16[256,768]{1,0:T(8,128)(2,1)S(1)}, bf16[256,768]{1,0:T(8,128)(2,1)S(1)}, u32[]{:S(2)}, u32[]{:S(2)}) collective-permute-start(bf16[256,768]{1,0:T(8,128)(2,1)S(1)} %collective-permute-done.27.refs_2_), channel_id=1, source_target_pairs={{0,8},{4,12},{8,16},{12,20},{16,24},{20,28},{24,0},{28,4},{1,9},{5... | collective-permute-start | bytes 1179656 | tf_op jit(solution)/shard_map/ppermute | solution.py:423
  83.6 24.8 %collective-permute-start.17 = (bf16[256,768]{1,0:T(8,128)(2,1)}, bf16[256,768]{1,0:T(8,128)(2,1)}, u32[]{:S(2)}, u32[]{:S(2)}) collective-permute-start(bf16[256,768]{1,0:T(8,128)(2,1)} %collective-permute-done.15.refs_10_), channel_id=1, source_target_pairs={{0,8},{4,12},{8,16},{12,20},{16,24},{20,28},{24,0},{28,4},{1,9},{5... | collective-permute-start | bytes 1179656 | tf_op jit(solution)/shard_map/ppermute | solution.py:423
  91.6 20.0 %collective-permute-start.16 = (bf16[256,768]{1,0:T(8,128)(2,1)}, bf16[256,768]{1,0:T(8,128)(2,1)S(1)}, u32[]{:S(2)}, u32[]{:S(2)}) collective-permute-start(bf16[256,768]{1,0:T(8,128)(2,1)} %collective-permute-done.15.refs_10_), channel_id=1, source_target_pairs={{0,4},{4,0},{8,12},{12,8},{16,20},{20,16},{24,28},{28,24},{1,5},{5... | collective-permute-start | bytes 1179656 | tf_op jit(solution)/shard_map/ppermute | solution.py:427
  99.9 16.9 %collective-permute-start.24 = (bf16[256,768]{1,0:T(8,128)(2,1)}, bf16[256,768]{1,0:T(8,128)(2,1)S(1)}, u32[]{:S(2)}, u32[]{:S(2)}) collective-permute-start(bf16[256,768]{1,0:T(8,128)(2,1)} %collective-permute-done.22.refs_4_), channel_id=1, source_target_pairs={{0,8},{4,12},{8,16},{12,20},{16,24},{20,28},{24,0},{28,4},{1,9},{5... | collective-permute-start | bytes 1179656 | tf_op jit(solution)/shard_map/ppermute | solution.py:423
  108.4 15.8 %collective-permute-start.32 = (bf16[256,768]{1,0:T(8,128)(2,1)S(1)}, bf16[256,768]{1,0:T(8,128)(2,1)S(1)}, u32[]{:S(2)}, u32[]{:S(2)}) collective-permute-start(bf16[256,768]{1,0:T(8,128)(2,1)S(1)} %collective-permute-done.28.refs_3_), channel_id=1, source_target_pairs={{0,8},{4,12},{8,16},{12,20},{16,24},{20,28},{24,0},{28,4},{1,9},{5... | collective-permute-start | bytes 1179656 | tf_op jit(solution)/shard_map/ppermute | solution.py:423
  108.4 16.5 %collective-permute-start.18 = (bf16[256,768]{1,0:T(8,128)(2,1)}, bf16[256,768]{1,0:T(8,128)(2,1)S(1)}, u32[]{:S(2)}, u32[]{:S(2)}) collective-permute-start(bf16[256,768]{1,0:T(8,128)(2,1)} %collective-permute-done.17.refs_12_), channel_id=1, source_target_pairs={{0,4},{4,0},{8,12},{12,8},{16,20},{20,16},{24,28},{28,24},{1,5},{5... | collective-permute-start | bytes 1179656 | tf_op jit(solution)/shard_map/ppermute | solution.py:427
  109.9 22.1 %collective-permute-start.11 = (bf16[128,2048]{1,0:T(8,128)(2,1)}, bf16[128,2048]{1,0:T(8,128)(2,1)S(1)}, u32[]{:S(2)}, u32[]{:S(2)}) collective-permute-start(bf16[128,2048]{1,0:T(8,128)(2,1)} %collective-permute-done.10.refs_4_), channel_id=1, source_target_pairs={{0,1},{1,0},{2,3},{3,2},{4,5},{5,4},{6,7},{7,6},{8,9},{9,8},{10,11... | collective-permute-start | bytes 1572872 | tf_op jit(solution)/shard_map/ppermute | solution.py:416
  109.9 40.5 %copy-start.27 = (f32[3,768]{1,0:T(4,128)S(1)}, f32[3,768]{1,0:T(4,128)}, u32[]{:S(2)}) copy-start(f32[3,768]{1,0:T(4,128)} %gate_taps.1) | copy-start | bytes 27652
  109.9 40.5 %copy-start.28 = (f32[3,768]{1,0:T(4,128)S(1)}, f32[3,768]{1,0:T(4,128)}, u32[]{:S(2)}) copy-start(f32[3,768]{1,0:T(4,128)} %value_taps.1) | copy-start | bytes 27652
  111.5 38.8 %collective-permute-start.23 = (bf16[256,768]{1,0:T(8,128)(2,1)}, bf16[256,768]{1,0:T(8,128)(2,1)S(1)}, u32[]{:S(2)}, u32[]{:S(2)}) collective-permute-start(bf16[256,768]{1,0:T(8,128)(2,1)} %collective-permute-done.22.refs_4_), channel_id=1, source_target_pairs={{0,4},{4,0},{8,12},{12,8},{16,20},{20,16},{24,28},{28,24},{1,5},{5... | collective-permute-start | bytes 1179656 | tf_op jit(solution)/shard_map/ppermute | solution.py:427
  116.7 33.6 %collective-permute-start.25 = (bf16[256,768]{1,0:T(8,128)(2,1)S(1)}, bf16[256,768]{1,0:T(8,128)(2,1)S(1)}, u32[]{:S(2)}, u32[]{:S(2)}) collective-permute-start(bf16[256,768]{1,0:T(8,128)(2,1)S(1)} %collective-permute-done.24.refs_6_), channel_id=1, source_target_pairs={{0,4},{4,0},{8,12},{12,8},{16,20},{20,16},{24,28},{28,24},{1,5},{5... | collective-permute-start | bytes 1179656 | tf_op jit(solution)/shard_map/ppermute | solution.py:427
  124.2 2.8 %collective-permute-start.8 = (bf16[16,2048]{1,0:T(8,128)(2,1)S(1)}, bf16[16,2048]{1,0:T(8,128)(2,1)S(1)}, u32[]{:S(2)}, u32[]{:S(2)}) collective-permute-start(bf16[16,2048]{1,0:T(8,128)(2,1)S(1)} %slice_select_fusion), channel_id=1, source_target_pairs={{2,4},{3,5},{6,8},{7,9},{10,12},{11,13},{14,16},{15,17},{18,20},{1... | collective-permute-start | bytes 196616 | tf_op jit(solution)/shard_map/ppermute | solution.py:497
  124.9 31.2 %collective-permute-start.33 = (bf16[256,768]{1,0:T(8,128)(2,1)S(1)}, bf16[256,768]{1,0:T(8,128)(2,1)S(1)}, u32[]{:S(2)}, u32[]{:S(2)}) collective-permute-start(bf16[256,768]{1,0:T(8,128)(2,1)S(1)} %collective-permute-done.28.refs_3_), channel_id=1, source_target_pairs={{0,4},{4,0},{8,12},{12,8},{16,20},{20,16},{24,28},{28,24},{1,5},{5... | collective-permute-start | bytes 1179656 | tf_op jit(solution)/shard_map/ppermute | solution.py:427
  127.0 0.7 collective-permute-start.9
  127.7 33.3 %collective-permute-start.37 = (bf16[256,768]{1,0:T(8,128)(2,1)S(1)}, bf16[256,768]{1,0:T(8,128)(2,1)S(1)}, u32[]{:S(2)}, u32[]{:S(2)}) collective-permute-start(bf16[256,768]{1,0:T(8,128)(2,1)S(1)} %collective-permute-done.26.refs_1_), channel_id=1, source_target_pairs={{0,8},{4,12},{8,16},{12,20},{16,24},{20,28},{24,0},{28,4},{1,9},{5... | collective-permute-start | bytes 1179656 | tf_op jit(solution)/shard_map/ppermute | solution.py:425
  132.0 29.7 %collective-permute-start.38 = (bf16[256,768]{1,0:T(8,128)(2,1)S(1)}, bf16[256,768]{1,0:T(8,128)(2,1)S(1)}, u32[]{:S(2)}, u32[]{:S(2)}) collective-permute-start(bf16[256,768]{1,0:T(8,128)(2,1)S(1)} %collective-permute-done.32.refs_0_), channel_id=1, source_target_pairs={{0,4},{4,0},{8,12},{12,8},{16,20},{20,16},{24,28},{28,24},{1,5},{5... | collective-permute-start | bytes 1179656 | tf_op jit(solution)/shard_map/ppermute | solution.py:427
  146.1 4.3 %copy-start.18 = (bf16[256,768]{1,0:T(8,128)(2,1)S(1)}, bf16[256,768]{1,0:T(8,128)(2,1)}, u32[]{:S(2)}) copy-start(bf16[256,768]{1,0:T(8,128)(2,1)} %copy-done.17) | copy-start | bytes 1179652
  146.1 4.3 %copy-start.20 = (bf16[256,768]{1,0:T(8,128)(2,1)S(1)}, bf16[256,768]{1,0:T(8,128)(2,1)}, u32[]{:S(2)}) copy-start(bf16[256,768]{1,0:T(8,128)(2,1)} %copy-done.19) | copy-start | bytes 1179652
  157.1 6.5 %collective-permute-start.34 = (bf16[128,512]{1,0:T(8,128)(2,1)S(1)}, bf16[128,512]{1,0:T(8,128)(2,1)S(1)}, u32[]{:S(2)}, u32[]{:S(2)}) collective-permute-start(bf16[128,512]{1,0:T(8,128)(2,1)S(1)} %get-tuple-element.50), channel_id=1, source_target_pairs={{0,1},{1,0},{2,3},{3,2},{4,5},{5,4},{6,7},{7,6},{8,9},{9,8},{10,11... | collective-permute-start | bytes 393224 | tf_op jit(solution)/shard_map/ppermute | solution.py:416
  158.3 5.9 %collective-permute-start.29 = (bf16[128,1024]{1,0:T(8,128)(2,1)S(1)}, bf16[128,1024]{1,0:T(8,128)(2,1)S(1)}, u32[]{:S(2)}, u32[]{:S(2)}) collective-permute-start(bf16[128,1024]{1,0:T(8,128)(2,1)S(1)} %get-tuple-element.46), channel_id=1, source_target_pairs={{0,1},{1,0},{2,3},{3,2},{4,5},{5,4},{6,7},{7,6},{8,9},{9,8},{10,11... | collective-permute-start | bytes 786440 | tf_op jit(solution)/shard_map/ppermute | solution.py:416
  160.0 13.7 %collective-permute-start.31 = (bf16[128,1024]{1,0:T(8,128)(2,1)S(1)}, bf16[128,1024]{1,0:T(8,128)(2,1)S(1)}, u32[]{:S(2)}, u32[]{:S(2)}) collective-permute-start(bf16[128,1024]{1,0:T(8,128)(2,1)S(1)} %get-tuple-element.48), channel_id=1, source_target_pairs={{0,1},{1,0},{2,3},{3,2},{4,5},{5,4},{6,7},{7,6},{8,9},{9,8},{10,11... | collective-permute-start | bytes 786440 | tf_op jit(solution)/shard_map/ppermute | solution.py:416
  161.0 22.5 %copy-start.14 = (bf16[128,2048]{1,0:T(8,128)(2,1)S(1)}, bf16[128,2048]{1,0:T(8,128)(2,1)}, u32[]{:S(2)}) copy-start(bf16[128,2048]{1,0:T(8,128)(2,1)} %copy-done.13) | copy-start | bytes 1572868
  161.1 22.5 %copy-start.31 = (f32[2048]{0:T(1024)S(1)}, f32[2048]{0:T(1024)}, u32[]{:S(2)}) copy-start(f32[2048]{0:T(1024)} %param.31) | copy-start | bytes 24580
  161.1 10.6 %collective-permute-start.36 = (bf16[128,512]{1,0:T(8,128)(2,1)S(1)}, bf16[128,512]{1,0:T(8,128)(2,1)S(1)}, u32[]{:S(2)}, u32[]{:S(2)}) collective-permute-start(bf16[128,512]{1,0:T(8,128)(2,1)S(1)} %get-tuple-element.52), channel_id=1, source_target_pairs={{0,1},{1,0},{2,3},{3,2},{4,5},{5,4},{6,7},{7,6},{8,9},{9,8},{10,11... | collective-permute-start | bytes 393224 | tf_op jit(solution)/shard_map/ppermute | solution.py:416
  162.6 9.0 %collective-permute-start.39 = (bf16[128,512]{1,0:T(8,128)(2,1)S(1)}, bf16[128,512]{1,0:T(8,128)(2,1)S(1)}, u32[]{:S(2)}, u32[]{:S(2)}) collective-permute-start(bf16[128,512]{1,0:T(8,128)(2,1)S(1)} %get-tuple-element.54), channel_id=1, source_target_pairs={{0,1},{1,0},{2,3},{3,2},{4,5},{5,4},{6,7},{7,6},{8,9},{9,8},{10,11... | collective-permute-start | bytes 393224 | tf_op jit(solution)/shard_map/ppermute | solution.py:416
  163.6 10.1 %collective-permute-start.41 = (bf16[128,512]{1,0:T(8,128)(2,1)S(1)}, bf16[128,512]{1,0:T(8,128)(2,1)S(1)}, u32[]{:S(2)}, u32[]{:S(2)}) collective-permute-start(bf16[128,512]{1,0:T(8,128)(2,1)S(1)} %get-tuple-element.56), channel_id=1, source_target_pairs={{0,1},{1,0},{2,3},{3,2},{4,5},{5,4},{6,7},{7,6},{8,9},{9,8},{10,11... | collective-permute-start | bytes 393224 | tf_op jit(solution)/shard_map/ppermute | solution.py:416
  164.2 11.6 %collective-permute-start.35 = (bf16[128,512]{1,0:T(8,128)(2,1)S(1)}, bf16[128,512]{1,0:T(8,128)(2,1)S(1)}, u32[]{:S(2)}, u32[]{:S(2)}) collective-permute-start(bf16[128,512]{1,0:T(8,128)(2,1)S(1)} %add_convert_fusion.2), channel_id=1, source_target_pairs={{0,2},{1,3},{2,0},{3,1},{4,6},{5,7},{6,4},{7,5},{8,10},{9,11},{10,... | collective-permute-start | bytes 393224 | tf_op jit(solution)/shard_map/ppermute | solution.py:539
  171.5 12.0 %collective-permute-start.30 = (bf16[128,1024]{1,0:T(8,128)(2,1)S(1)}, bf16[128,1024]{1,0:T(8,128)(2,1)S(1)}, u32[]{:S(2)}, u32[]{:S(2)}) collective-permute-start(bf16[128,1024]{1,0:T(8,128)(2,1)S(1)} %add_convert_fusion), channel_id=1, source_target_pairs={{0,2},{1,3},{2,0},{3,1},{4,6},{5,7},{6,4},{7,5},{8,10},{9,11},{10,... | collective-permute-start | bytes 786440 | tf_op jit(solution)/shard_map/ppermute | solution.py:539
  171.7 11.9 %collective-permute-start.40 = (bf16[128,512]{1,0:T(8,128)(2,1)S(1)}, bf16[128,512]{1,0:T(8,128)(2,1)S(1)}, u32[]{:S(2)}, u32[]{:S(2)}) collective-permute-start(bf16[128,512]{1,0:T(8,128)(2,1)S(1)} %add_convert_fusion.1), channel_id=1, source_target_pairs={{0,2},{1,3},{2,0},{3,1},{4,6},{5,7},{6,4},{7,5},{8,10},{9,11},{10,... | collective-permute-start | bytes 393224 | tf_op jit(solution)/shard_map/ppermute | solution.py:539
  (15 other events, 16.7 us)
where the time goes:
time: 186 us
  waiting for transfers between devices  77.8 us (42%)
  starting transfers between devices  65.8 us (35%)
  Pallas kernels  28.8 us (15%)
  local copies, waits for them, and re-layouts  12.4 us (7%)
    ppermute x9, waiting for transfers between devices, spread(): found[k, 0] = lax.ppermute(found[k - 1, 0], 'sp', ring)  54 us
    pallas_call x18, Pallas kernels, call(): pl.pallas_call(kernel, out_shape=tuple((jax.ShapeDtypeStruct(*o) for o in...  28.8 us
    ppermute x11, starting transfers between devices, spread(): found[k, 1] = lax.ppermute(found[k, 0], 'sp', swap)  23.5 us
    unnamed x74, local copies, waits for them, and re-layouts  12.4 us
    ppermute x3, waiting for transfers between devices, layer(): parts[g].append(lax.ppermute(both, 'tp', route))  9.82 us
    ppermute x9, starting transfers between devices, spread(): found[k, 0] = lax.ppermute(found[k - 1, 0], 'sp', ring)  9.45 us
    ppermute x3, starting transfers between devices, layer(): parts[g].append(lax.ppermute(both, 'tp', route))  9.39 us
    ppermute x2, starting transfers between devices, layer(): states.insert(0, lax.ppermute(total, 'sp', route))  9.28 us
  transfers between devices with their start and end apart: 42, of which 16 were waited for; matrix products, arithmetic and copies ran while one was open for 0% of the time, Pallas kernels for 14%

commit v1 on v0

--- a/solution.py
+++ b/solution.py
@@ -352,6 +352,10 @@
         keep_out[:, start:end] = product[:step]
         send_out[:, start:end] = product[step:]
         start = end
+
+
+def add_kernel(info, mine, theirs, out):
+    out[...] = (mine[...].astype(f32) + theirs[...].astype(f32)).astype(bf16)
 
 
 def result_kernel(groups, rows, nz, pair, info, stream, post_gain, *refs):
@@ -520,7 +524,7 @@
         scratch=(pltpu.VMEM((2, PAD + rows, width), f32),),
     )
     arrival = sorted(order, key=lambda o: o[0] + o[1] * {0: 1, 1: nz + 1}.get(o[0], nz - 1))
-    cuts = [len(arrival) * i // 4 for i in (0, 2, 3, 4)]
+    cuts = [len(arrival) * i // 8 for i in (0, 4, 7, 8)]
     groups = [arrival[a:b] for a, b in zip(cuts, cuts[1:]) if b > a]
     rows_of = model // len(order)
     parts = [[] for _ in groups]
@@ -534,7 +538,7 @@
             )
             theirs = mate(away)
             if d:
-                both = (mine.astype(f32) + theirs.astype(f32)).astype(bf16)
+                both = call(add_kernel, shape, (info, mine, theirs))
                 route = [(i, (i + 2 * d) % n_tp) for i in range(n_tp)]
                 parts[g].append(lax.ppermute(both, "tp", route))
             else:

time: 186 us -> 172 us (0.925)
  starting transfers between devices: 65.8 us -> 50.8 us
    ppermute x3, starting transfers between devices: 9.39 us -> 3.35 us  [layer(): parts[g].append(lax.ppermute(both, 'tp', route))]
    ppermute x11, waiting for transfers between devices: 2.15 us -> 6.98 us  [spread(): found[k, 1] = lax.ppermute(found[k, 0], 'sp', swap)]
    ppermute x11, starting transfers between devices: 23.5 us -> 19 us  [spread(): found[k, 1] = lax.ppermute(found[k, 0], 'sp', swap)]
    ppermute x3, waiting for transfers between devices: 9.82 us -> 5.7 us  [layer(): parts[g].append(lax.ppermute(both, 'tp', route))]
    ppermute x9, starting transfers between devices: 9.45 us -> 6.09 us  [spread(): found[k, 0] = lax.ppermute(found[k - 1, 0], 'sp', ring)]
    pallas_call x18 -> x21, Pallas kernels: 28.8 us -> 30.5 us  [call(): pl.pallas_call(kernel, out_shape=tuple((jax.ShapeDtypeStruct(*o) for o in...]
    unnamed x74 -> x70, local copies, waits for them, and re-layouts: 12.4 us -> 11 us
  transfers between devices with their start and end apart: 42 -> 42, of which waited for: 16 -> 18; matrix products, arithmetic and copies ran while one was open for 0% -> 0% of each run, Pallas kernels for 14% -> 17%
where the time goes in v1:
time: 172 us
  waiting for transfers between devices  78.9 us (46%)
  starting transfers between devices  50.8 us (30%)
  Pallas kernels  30.5 us (18%)
  local copies, waits for them, and re-layouts  11 us (6%)
    ppermute x9, waiting for transfers between devices, spread(): found[k, 0] = lax.ppermute(found[k - 1, 0], 'sp', ring)  52.8 us
    pallas_call x21, Pallas kernels, call(): pl.pallas_call(kernel, out_shape=tuple((jax.ShapeDtypeStruct(*o) for o in...  30.5 us
    ppermute x11, starting transfers between devices, spread(): found[k, 1] = lax.ppermute(found[k, 0], 'sp', swap)  19 us
    unnamed x70, local copies, waits for them, and re-layouts  11 us
    ppermute x2, starting transfers between devices, layer(): states.insert(0, lax.ppermute(total, 'sp', route))  9.28 us
    ppermute x11, waiting for transfers between devices, spread(): found[k, 1] = lax.ppermute(found[k, 0], 'sp', swap)  6.98 us
    ppermute x9, starting transfers between devices, spread(): found[k, 0] = lax.ppermute(found[k - 1, 0], 'sp', ring)  6.09 us
    ppermute x3, waiting for transfers between devices, layer(): parts[g].append(lax.ppermute(both, 'tp', route))  5.7 us
  transfers between devices with their start and end apart: 42, of which 18 were waited for; matrix products, arithmetic and copies ran while one was open for 0% of the time, Pallas kernels for 17%

profile of v1, /device:TPU:0, one launch (start us, length us, event | category | flops | bytes accessed | tf_op | source)
XLA Modules:
  0.0 171.8 jit_solution(8072686190220689847)
XLA Ops:
  0.5 1.0 copy-done.1
  1.5 0.9 copy-done.6
  2.5 0.7 copy-done.30
  3.9 1.8 %shard_map.155 = (bf16[1,144,512]{2,1,0:T(8,128)(2,1)S(1)}, bf16[1,144,512]{2,1,0:T(8,128)(2,1)S(1)}) custom-call(s32[8]{0:T(128)S(1)} %compare_select_fusion.2.info, bf16[512,256]{1,0:T(8,128)(2,1)S(1)} %copy-done.6, bf16[512,512]{1,0:T(8,128)(2,1)S(1)} %copy-done.1, f32[1,512]{1,0:T(1,128)S(1)} %copy-done.30, f32[1,512]{1,0:T(1,128)S(1)} %copy-done.32), custom_call_target="tpu_custom_call" | custom-call | tf_op jit(solution)/shard_map/pallas_call | solution.py:33
  5.7 2.6 %collective-permute-start = (bf16[1,144,512]{2,1,0:T(8,128)(2,1)S(1)}, bf16[1,144,512]{2,1,0:T(8,128)(2,1)S(1)}, u32[]{:S(2)}, u32[]{:S(2)}) collective-permute-start(bf16[1,144,512]{2,1,0:T(8,128)(2,1)S(1)} %get-tuple-element.34), channel_id=1, source_target_pairs={{0,4},{4,0},{8,12},{12,8},{16,20},{20,16},{24,28},{28,24},{1,5},{5... | collective-permute-start | bytes 442376 | tf_op jit(solution)/shard_map/ppermute | solution.py:457
  8.3 4.5 %collective-permute-done.theirs = bf16[1,144,512]{2,1,0:T(8,128)(2,1)S(1)} collective-permute-done((bf16[1,144,512]{2,1,0:T(8,128)(2,1)S(1)}, bf16[1,144,512]{2,1,0:T(8,128)(2,1)S(1)}, u32[]{:S(2)}, u32[]{:S(2)}) %collective-permute-start) | collective-permute-done | bytes 147488 | tf_op jit(solution)/shard_map/ppermute | solution.py:457
  13.4 3.7 %collective-permute-start.1 = (bf16[1,144,512]{2,1,0:T(8,128)(2,1)S(1)}, bf16[1,144,512]{2,1,0:T(8,128)(2,1)S(1)}, u32[]{:S(2)}, u32[]{:S(2)}) collective-permute-start(bf16[1,144,512]{2,1,0:T(8,128)(2,1)S(1)} %shard_map.156.later), channel_id=1, source_target_pairs={{0,8},{4,12},{8,16},{12,20},{16,24},{20,28},{1,9},{5,13},{9,17},{1... | collective-permute-start | bytes 442376 | tf_op jit(solution)/shard_map/ppermute | solution.py:463
  17.2 2.8 %collective-permute-done.1.earlier.refs_1_ = bf16[1,144,512]{2,1,0:T(8,128)(2,1)S(1)} collective-permute-done((bf16[1,144,512]{2,1,0:T(8,128)(2,1)S(1)}, bf16[1,144,512]{2,1,0:T(8,128)(2,1)S(1)}, u32[]{:S(2)}, u32[]{:S(2)}) %collective-permute-start.1) | collective-permute-done | bytes 147488 | tf_op jit(solution)/shard_map/ppermute | solution.py:463
  20.7 5.5 %collective-permute-start.2 = (bf16[1,144,512]{2,1,0:T(8,128)(2,1)S(1)}, bf16[1,144,512]{2,1,0:T(8,128)(2,1)S(1)}, u32[]{:S(2)}, u32[]{:S(2)}) collective-permute-start(bf16[1,144,512]{2,1,0:T(8,128)(2,1)S(1)} %shard_map.157), channel_id=1, source_target_pairs={{0,16},{4,20},{8,24},{12,28},{1,17},{5,21},{9,25},{13,29},{2,18},{... | collective-permute-start | bytes 442376 | tf_op jit(solution)/shard_map/ppermute | solution.py:463
  26.3 2.7 %collective-permute-done.2.refs_0_ = bf16[1,144,512]{2,1,0:T(8,128)(2,1)S(1)} collective-permute-done((bf16[1,144,512]{2,1,0:T(8,128)(2,1)S(1)}, bf16[1,144,512]{2,1,0:T(8,128)(2,1)S(1)}, u32[]{:S(2)}, u32[]{:S(2)}) %collective-permute-start.2) | collective-permute-done | bytes 147488 | tf_op jit(solution)/shard_map/ppermute | solution.py:463
  28.9 0.8 shard_map.158
  29.7 1.6 collective-permute-start.3
  31.8 1.9 %shard_map.154 = (f32[512,512]{1,0:T(8,128)S(1)}, f32[1,512,128]{2,1,0:T(8,128)S(1)}) custom-call(s32[8]{0:T(128)S(1)} %compare_select_fusion.2.info, bf16[512,256]{1,0:T(8,128)(2,1)S(1)} %copy-done.8, bf16[512,256]{1,0:T(8,128)(2,1)S(1)} %copy-done.7, bf16[512,512]{1,0:T(8,128)(2,1)S(1)} %copy-done.2, f32[1,512]{1,0:T(1,128)S(1)} %copy-done.31, ...), custom_call_target="tpu_custom_call" | custom-call | tf_op jit(solution)/shard_map/pallas_call | solution.py:33
  33.7 2.8 %collective-permute-done.3.theirs = bf16[1,144,512]{2,1,0:T(8,128)(2,1)S(1)} collective-permute-done((bf16[1,144,512]{2,1,0:T(8,128)(2,1)S(1)}, bf16[1,144,512]{2,1,0:T(8,128)(2,1)S(1)}, u32[]{:S(2)}, u32[]{:S(2)}) %collective-permute-start.3) | collective-permute-done | bytes 147488 | tf_op jit(solution)/shard_map/ppermute | solution.py:468
  36.5 1.4 shard_map.159
  38.0 4.0 %collective-permute-start.13 = (bf16[256,768]{1,0:T(8,128)(2,1)S(1)}, bf16[256,768]{1,0:T(8,128)(2,1)S(1)}, u32[]{:S(2)}, u32[]{:S(2)}) collective-permute-start(bf16[256,768]{1,0:T(8,128)(2,1)S(1)} %copy-done.34), channel_id=1, source_target_pairs={{0,8},{4,12},{8,16},{12,20},{16,24},{20,28},{24,0},{28,4},{1,9},{5... | collective-permute-start | bytes 1179656 | tf_op jit(solution)/shard_map/ppermute | solution.py:427
  42.0 1.3 shard_map.160
  43.3 1.6 collective-permute-start.6
  44.9 1.5 collective-permute-start.19
  46.4 1.4 collective-permute-start.20
  47.9 0.7 copy-done.19
  49.2 5.6 %collective-permute-done.13.refs_8_ = bf16[256,768]{1,0:T(8,128)(2,1)S(1)} collective-permute-done((bf16[256,768]{1,0:T(8,128)(2,1)S(1)}, bf16[256,768]{1,0:T(8,128)(2,1)S(1)}, u32[]{:S(2)}, u32[]{:S(2)}) %collective-permute-start.13) | collective-permute-done | bytes 393248 | tf_op jit(solution)/shard_map/ppermute | solution.py:427
  54.8 2.1 %collective-permute-done.19.refs_1_ = bf16[256,768]{1,0:T(8,128)(2,1)S(1)} collective-permute-done((bf16[256,768]{1,0:T(8,128)(2,1)S(1)}, bf16[256,768]{1,0:T(8,128)(2,1)S(1)}, u32[]{:S(2)}, u32[]{:S(2)}) %collective-permute-start.19) | collective-permute-done | bytes 393248 | tf_op jit(solution)/shard_map/ppermute | solution.py:431
  56.9 0.7 copy-done.13
  57.7 1.5 collective-permute-start.14
  59.2 4.0 %collective-permute-done.20.refs_2_ = bf16[256,768]{1,0:T(8,128)(2,1)S(1)} collective-permute-done((bf16[256,768]{1,0:T(8,128)(2,1)S(1)}, bf16[256,768]{1,0:T(8,128)(2,1)S(1)}, u32[]{:S(2)}, u32[]{:S(2)}) %collective-permute-start.20) | collective-permute-done | bytes 393248 | tf_op jit(solution)/shard_map/ppermute | solution.py:427
  63.2 0.8 copy-done.21
  64.0 1.4 collective-permute-done.26.refs_1_
  65.4 1.5 collective-permute-start.21
  66.8 4.8 %collective-permute-done.27.refs_2_ = bf16[256,768]{1,0:T(8,128)(2,1)S(1)} collective-permute-done((bf16[256,768]{1,0:T(8,128)(2,1)S(1)}, bf16[256,768]{1,0:T(8,128)(2,1)S(1)}, u32[]{:S(2)}, u32[]{:S(2)}) %collective-permute-start.27) | collective-permute-done | bytes 393248 | tf_op jit(solution)/shard_map/ppermute | solution.py:427
  72.3 1.3 shard_map.161.refs_1_
  73.6 1.1 shard_map.162
  74.7 0.7 copy-done.23
  75.5 4.7 %collective-permute-done.15.refs_10_ = bf16[256,768]{1,0:T(8,128)(2,1)} collective-permute-done((bf16[256,768]{1,0:T(8,128)(2,1)S(1)}, bf16[256,768]{1,0:T(8,128)(2,1)}, u32[]{:S(2)}, u32[]{:S(2)}) %collective-permute-start.15) | collective-permute-done | bytes 393248 | tf_op jit(solution)/shard_map/ppermute | solution.py:427
  80.2 1.5 collective-permute-start.10
  81.7 0.8 copy-done.17
  82.4 1.5 collective-permute-start.16
  83.9 4.7 %collective-permute-done.22.refs_4_ = bf16[256,768]{1,0:T(8,128)(2,1)} collective-permute-done((bf16[256,768]{1,0:T(8,128)(2,1)S(1)}, bf16[256,768]{1,0:T(8,128)(2,1)}, u32[]{:S(2)}, u32[]{:S(2)}) %collective-permute-start.22) | collective-permute-done | bytes 393248 | tf_op jit(solution)/shard_map/ppermute | solution.py:427
  88.6 8.3 %collective-permute-done.28.refs_3_ = bf16[256,768]{1,0:T(8,128)(2,1)S(1)} collective-permute-done((bf16[256,768]{1,0:T(8,128)(2,1)S(1)}, bf16[256,768]{1,0:T(8,128)(2,1)S(1)}, u32[]{:S(2)}, u32[]{:S(2)}) %collective-permute-start.28) | collective-permute-done | bytes 393248 | tf_op jit(solution)/shard_map/ppermute | solution.py:427
  96.9 0.8 copy-done.4
  97.7 1.5 collective-permute-start.23
  99.2 6.3 %collective-permute-done.17.refs_12_ = bf16[256,768]{1,0:T(8,128)(2,1)} collective-permute-done((bf16[256,768]{1,0:T(8,128)(2,1)}, bf16[256,768]{1,0:T(8,128)(2,1)}, u32[]{:S(2)}, u32[]{:S(2)}) %collective-permute-start.17) | collective-permute-done | bytes 393248 | tf_op jit(solution)/shard_map/ppermute | solution.py:427
  105.4 8.4 %collective-permute-done.24.refs_6_ = bf16[256,768]{1,0:T(8,128)(2,1)} collective-permute-done((bf16[256,768]{1,0:T(8,128)(2,1)}, bf16[256,768]{1,0:T(8,128)(2,1)}, u32[]{:S(2)}, u32[]{:S(2)}) %collective-permute-start.24) | collective-permute-done | bytes 393248 | tf_op jit(solution)/shard_map/ppermute | solution.py:427
  113.9 1.5 collective-permute-start.18
  116.0 6.0 %collective-permute-done.32.refs_0_ = bf16[256,768]{1,0:T(8,128)(2,1)S(1)} collective-permute-done((bf16[256,768]{1,0:T(8,128)(2,1)}, bf16[256,768]{1,0:T(8,128)(2,1)S(1)}, u32[]{:S(2)}, u32[]{:S(2)}) %collective-permute-start.32) | collective-permute-done | bytes 393248 | tf_op jit(solution)/shard_map/ppermute | solution.py:427
  122.6 3.5 %collective-permute-done.18.refs_13_ = bf16[256,768]{1,0:T(8,128)(2,1)S(1)} collective-permute-done((bf16[256,768]{1,0:T(8,128)(2,1)}, bf16[256,768]{1,0:T(8,128)(2,1)S(1)}, u32[]{:S(2)}, u32[]{:S(2)}) %collective-permute-start.18) | collective-permute-done | bytes 393248 | tf_op jit(solution)/shard_map/ppermute | solution.py:431
  126.7 2.6 %collective-permute-start.34 = (bf16[256,768]{1,0:T(8,128)(2,1)S(1)}, bf16[256,768]{1,0:T(8,128)(2,1)S(1)}, u32[]{:S(2)}, u32[]{:S(2)}) collective-permute-start(bf16[256,768]{1,0:T(8,128)(2,1)S(1)} %collective-permute-done.26.refs_1_), channel_id=1, source_target_pairs={{0,8},{4,12},{8,16},{12,20},{16,24},{20,28},{24,0},{28,4},{1,9},{5... | collective-permute-start | bytes 1179656 | tf_op jit(solution)/shard_map/ppermute | solution.py:429
  129.4 8.3 %collective-permute-start.33 = (bf16[256,768]{1,0:T(8,128)(2,1)}, bf16[256,768]{1,0:T(8,128)(2,1)S(1)}, u32[]{:S(2)}, u32[]{:S(2)}) collective-permute-start(bf16[256,768]{1,0:T(8,128)(2,1)} %copy-done.4), channel_id=1, source_target_pairs={{0,4},{4,0},{8,12},{12,8},{16,20},{20,16},{24,28},{28,24},{1,5},{5... | collective-permute-start | bytes 1179656 | tf_op jit(solution)/shard_map/ppermute | solution.py:431
  137.8 1.0 copy-done.20
  138.8 1.0 copy-done.22
  139.8 1.0 copy-done.24
  140.8 4.1 %shard_map.163 = (bf16[528,768]{1,0:T(8,128)(2,1)S(1)}, bf16[528,2048]{1,0:T(8,128)(2,1)S(1)}) custom-call(s32[8]{0:T(128)S(1)} %compare_select_fusion.2.info, bf16[16,2048]{1,0:T(8,128)(2,1)S(1)} %collective-permute-done.8.refs_0_, bf16[16,2048]{1,0:T(8,128)(2,1)S(1)} %collective-permute-done.9.refs_1_, bf16[128,2048]{1,0:T(8,128)(2,1)S(1)} %get-tuple-element.40.refs_2_, ...), custom_call_target="tpu_custom_call" | custom-call | tf_op jit(solution)/shard_map/pallas_call | solution.py:33
  145.0 5.7 %shard_map.164 = (bf16[2,128,768]{2,1,0:T(8,128)(2,1)S(1)}, bf16[2,128,768]{2,1,0:T(8,128)(2,1)S(1)}) custom-call(s32[8]{0:T(128)S(1)} %compare_select_fusion.2.info, f32[3,768]{1,0:T(4,128)S(1)} %copy-done.25, f32[3,768]{1,0:T(4,128)S(1)} %copy-done.26, bf16[528,2048]{1,0:T(8,128)(2,1)S(1)} %get-tuple-element.41.rows_all, ...), custom_call_target="tpu_custom_call" | custom-call | tf_op jit(solution)/shard_map/pallas_call | solution.py:33
  150.7 1.1 shard_map.165
  152.0 1.0 shard_map.168
  153.6 1.1 shard_map.167
  155.4 1.3 collective-permute-start.30
  156.7 0.8 shard_map.171
  157.8 1.0 shard_map.170
  159.8 0.9 collective-permute-start.36
  160.7 0.8 shard_map.173
  162.9 1.2 collective-permute-start.40
  164.1 5.7 %collective-permute-done.40.refs_6_ = bf16[128,256]{1,0:T(8,128)(2,1)S(1)} collective-permute-done((bf16[128,256]{1,0:T(8,128)(2,1)S(1)}, bf16[128,256]{1,0:T(8,128)(2,1)S(1)}, u32[]{:S(2)}, u32[]{:S(2)}) %collective-permute-start.40) | collective-permute-done | bytes 65568 | tf_op jit(solution)/shard_map/ppermute | solution.py:543
  169.8 2.0 %shard_map.174 = bf16[128,2048]{1,0:T(8,128)(2,1)} custom-call(s32[8]{0:T(128)S(1)} %compare_select_fusion.2.info, bf16[128,2048]{1,0:T(8,128)(2,1)S(1)} %get-tuple-element.39.stream, f32[1,2048]{1,0:T(1,128)S(1)} %bitcast.5, bf16[128,1024]{1,0:T(8,128)(2,1)S(1)} %collective-permute-done.30.refs_0_, bf16[128,1024]{1,0:T(8,128)(2,1)S(1)} %get-tuple-element.47.refs_1_, ...), custom_call_target="tpu_custom_call" | custom-call | tf_op jit(solution)/shard_map/pallas_call | solution.py:33
  (113 shorter events, 10.3 us)
Async XLA Ops:
  0.0 31.8 %copy-start.31 = (f32[1,512]{1,0:T(1,128)S(1)}, f32[1,512]{1,0:T(1,128)}, u32[]{:S(2)}) copy-start(f32[1,512]{1,0:T(1,128)} %ig.3) | copy-start | bytes 6148
  0.0 31.8 %copy-start.33 = (f32[1,512]{1,0:T(1,128)S(1)}, f32[1,512]{1,0:T(1,128)}, u32[]{:S(2)}) copy-start(f32[1,512]{1,0:T(1,128)} %fg.3) | copy-start | bytes 6148
  0.0 42.0 %collective-permute-start.5 = (bf16[512,2048]{1,0:T(8,128)(2,1)}, bf16[512,2048]{1,0:T(8,128)(2,1)S(1)}, u32[]{:S(2)}, u32[]{:S(2)}) collective-permute-start(bf16[512,2048]{1,0:T(8,128)(2,1)} %own_weight.3), channel_id=1, source_target_pairs={{0,1},{1,0},{2,3},{3,2},{4,5},{5,4},{6,7},{7,6},{8,9},{9,8},{10,11... | collective-permute-start | bytes 6291464 | tf_op jit(solution)/shard_map/ppermute | solution.py:420
  3.9 27.4 %copy-start.34 = (bf16[256,768]{1,0:T(8,128)(2,1)S(1)}, bf16[256,768]{1,0:T(8,128)(2,1)}, u32[]{:S(2)}) copy-start(bf16[256,768]{1,0:T(8,128)(2,1)} %refs_6_.1) | copy-start | bytes 1179652
  3.9 28.0 %copy-start.2 = (bf16[512,512]{1,0:T(8,128)(2,1)S(1)}, bf16[512,512]{1,0:T(8,128)(2,1)}, u32[]{:S(2)}) copy-start(bf16[512,512]{1,0:T(8,128)(2,1)} %value.3) | copy-start | bytes 1572868
  3.9 28.0 %copy-start.7 = (bf16[512,256]{1,0:T(8,128)(2,1)S(1)}, bf16[512,256]{1,0:T(8,128)(2,1)}, u32[]{:S(2)}) copy-start(bf16[512,256]{1,0:T(8,128)(2,1)} %key.3) | copy-start | bytes 786436
  3.9 28.0 %copy-start.8 = (bf16[512,256]{1,0:T(8,128)(2,1)S(1)}, bf16[512,256]{1,0:T(8,128)(2,1)}, u32[]{:S(2)}) copy-start(bf16[512,256]{1,0:T(8,128)(2,1)} %query.3) | copy-start | bytes 786436
  3.9 32.6 %copy-start.10 = (bf16[512,512]{1,0:T(8,128)(2,1)S(1)}, bf16[512,512]{1,0:T(8,128)(2,1)}, u32[]{:S(2)}) copy-start(bf16[512,512]{1,0:T(8,128)(2,1)} %out_gate.1) | copy-start | bytes 1572868
  5.7 7.1 %collective-permute-start = (bf16[1,144,512]{2,1,0:T(8,128)(2,1)S(1)}, bf16[1,144,512]{2,1,0:T(8,128)(2,1)S(1)}, u32[]{:S(2)}, u32[]{:S(2)}) collective-permute-start(bf16[1,144,512]{2,1,0:T(8,128)(2,1)S(1)} %get-tuple-element.34), channel_id=1, source_target_pairs={{0,4},{4,0},{8,12},{12,8},{16,20},{20,16},{24,28},{28,24},{1,5},{5... | collective-permute-start | bytes 442376 | tf_op jit(solution)/shard_map/ppermute | solution.py:457
  13.4 6.6 %collective-permute-start.1 = (bf16[1,144,512]{2,1,0:T(8,128)(2,1)S(1)}, bf16[1,144,512]{2,1,0:T(8,128)(2,1)S(1)}, u32[]{:S(2)}, u32[]{:S(2)}) collective-permute-start(bf16[1,144,512]{2,1,0:T(8,128)(2,1)S(1)} %shard_map.156.later), channel_id=1, source_target_pairs={{0,8},{4,12},{8,16},{12,20},{16,24},{20,28},{1,9},{5,13},{9,17},{1... | collective-permute-start | bytes 442376 | tf_op jit(solution)/shard_map/ppermute | solution.py:463
  20.7 21.3 %copy-start = (bf16[512,2048]{1,0:T(8,128)(2,1)S(1)}, bf16[512,2048]{1,0:T(8,128)(2,1)}, u32[]{:S(2)}) copy-start(bf16[512,2048]{1,0:T(8,128)(2,1)} %own_weight.3) | copy-start | bytes 6291460
  20.7 8.2 %collective-permute-start.2 = (bf16[1,144,512]{2,1,0:T(8,128)(2,1)S(1)}, bf16[1,144,512]{2,1,0:T(8,128)(2,1)S(1)}, u32[]{:S(2)}, u32[]{:S(2)}) collective-permute-start(bf16[1,144,512]{2,1,0:T(8,128)(2,1)S(1)} %shard_map.157), channel_id=1, source_target_pairs={{0,16},{4,20},{8,24},{12,28},{1,17},{5,21},{9,25},{13,29},{2,18},{... | collective-permute-start | bytes 442376 | tf_op jit(solution)/shard_map/ppermute | solution.py:463
  29.7 6.8 %collective-permute-start.3 = (bf16[1,144,512]{2,1,0:T(8,128)(2,1)S(1)}, bf16[1,144,512]{2,1,0:T(8,128)(2,1)S(1)}, u32[]{:S(2)}, u32[]{:S(2)}) collective-permute-start(bf16[1,144,512]{2,1,0:T(8,128)(2,1)S(1)} %get-tuple-element.36), channel_id=1, source_target_pairs={{0,4},{4,0},{8,12},{12,8},{16,20},{20,16},{24,28},{28,24},{1,5},{5... | collective-permute-start | bytes 442376 | tf_op jit(solution)/shard_map/ppermute | solution.py:468
  31.3 16.6 %collective-permute-start.12 = (bf16[256,768]{1,0:T(8,128)(2,1)S(1)}, bf16[256,768]{1,0:T(8,128)(2,1)S(1)}, u32[]{:S(2)}, u32[]{:S(2)}) collective-permute-start(bf16[256,768]{1,0:T(8,128)(2,1)S(1)} %copy-done.34), channel_id=1, source_target_pairs={{0,4},{4,0},{8,12},{12,8},{16,20},{20,16},{24,28},{28,24},{1,5},{5... | collective-permute-start | bytes 1179656 | tf_op jit(solution)/shard_map/ppermute | solution.py:431
  37.9 4.1 %collective-permute-start.4 = (bf16[2,128,512]{2,1,0:T(8,128)(2,1)S(1)}, bf16[2,128,512]{2,1,0:T(8,128)(2,1)S(1)}, u32[]{:S(2)}, u32[]{:S(2)}) collective-permute-start(bf16[2,128,512]{2,1,0:T(8,128)(2,1)S(1)} %get-tuple-element.38), channel_id=1, source_target_pairs={{0,1},{1,0},{2,3},{3,2},{4,5},{5,4},{6,7},{7,6},{8,9},{9,8},{10,11... | collective-permute-start | bytes 786440 | tf_op jit(solution)/shard_map/ppermute | solution.py:420
  38.0 16.8 %collective-permute-start.13 = (bf16[256,768]{1,0:T(8,128)(2,1)S(1)}, bf16[256,768]{1,0:T(8,128)(2,1)S(1)}, u32[]{:S(2)}, u32[]{:S(2)}) collective-permute-start(bf16[256,768]{1,0:T(8,128)(2,1)S(1)} %copy-done.34), channel_id=1, source_target_pairs={{0,8},{4,12},{8,16},{12,20},{16,24},{20,28},{24,0},{28,4},{1,9},{5... | collective-permute-start | bytes 1179656 | tf_op jit(solution)/shard_map/ppermute | solution.py:427
  42.0 2.9 %copy-start.11 = (bf16[256,768]{1,0:T(8,128)(2,1)S(1)}, bf16[256,768]{1,0:T(8,128)(2,1)}, u32[]{:S(2)}) copy-start(bf16[256,768]{1,0:T(8,128)(2,1)} %refs_0_.3) | copy-start | bytes 1179652
  42.0 6.6 %copy-start.3 = (bf16[256,768]{1,0:T(8,128)(2,1)S(1)}, bf16[256,768]{1,0:T(8,128)(2,1)}, u32[]{:S(2)}) copy-start(bf16[256,768]{1,0:T(8,128)(2,1)} %refs_0_.5) | copy-start | bytes 1179652
  43.3 30.3 %copy-start.9 = (bf16[128,2048]{1,0:T(8,128)(2,1)S(1)}, bf16[128,2048]{1,0:T(8,128)(2,1)}, u32[]{:S(2)}) copy-start(bf16[128,2048]{1,0:T(8,128)(2,1)} %residual.1) | copy-start | bytes 1572868
  43.3 30.3 %copy-start.27 = (f32[2048]{0:T(1024)S(1)}, f32[2048]{0:T(1024)}, u32[]{:S(2)}) copy-start(f32[2048]{0:T(1024)} %param.24) | copy-start | bytes 24580
  43.3 30.3 %copy-start.28 = (f32[2048]{0:T(1024)S(1)}, f32[2048]{0:T(1024)}, u32[]{:S(2)}) copy-start(f32[2048]{0:T(1024)} %param.25) | copy-start | bytes 24580
  43.3 28.3 %collective-permute-start.6 = (bf16[128,2048]{1,0:T(8,128)(2,1)S(1)}, bf16[128,2048]{1,0:T(8,128)(2,1)S(1)}, u32[]{:S(2)}, u32[]{:S(2)}) collective-permute-start(bf16[128,2048]{1,0:T(8,128)(2,1)S(1)} %shard_map.160), channel_id=1, source_target_pairs={{0,2},{1,3},{2,0},{3,1},{4,6},{5,7},{6,4},{7,5},{8,10},{9,11},{10,... | collective-permute-start | bytes 1572872 | tf_op jit(solution)/shard_map/ppermute | solution.py:421
  44.9 12.0 %collective-permute-start.19 = (bf16[256,768]{1,0:T(8,128)(2,1)S(1)}, bf16[256,768]{1,0:T(8,128)(2,1)S(1)}, u32[]{:S(2)}, u32[]{:S(2)}) collective-permute-start(bf16[256,768]{1,0:T(8,128)(2,1)S(1)} %copy-done.11), channel_id=1, source_target_pairs={{0,4},{4,0},{8,12},{12,8},{16,20},{20,16},{24,28},{28,24},{1,5},{5... | collective-permute-start | bytes 1179656 | tf_op jit(solution)/shard_map/ppermute | solution.py:431
  46.4 16.8 %collective-permute-start.20 = (bf16[256,768]{1,0:T(8,128)(2,1)S(1)}, bf16[256,768]{1,0:T(8,128)(2,1)S(1)}, u32[]{:S(2)}, u32[]{:S(2)}) collective-permute-start(bf16[256,768]{1,0:T(8,128)(2,1)S(1)} %copy-done.11), channel_id=1, source_target_pairs={{0,8},{4,12},{8,16},{12,20},{16,24},{20,28},{24,0},{28,4},{1,9},{5... | collective-permute-start | bytes 1179656 | tf_op jit(solution)/shard_map/ppermute | solution.py:427
  48.6 16.7 %collective-permute-start.26 = (bf16[256,768]{1,0:T(8,128)(2,1)S(1)}, bf16[256,768]{1,0:T(8,128)(2,1)S(1)}, u32[]{:S(2)}, u32[]{:S(2)}) collective-permute-start(bf16[256,768]{1,0:T(8,128)(2,1)S(1)} %copy-done.3), channel_id=1, source_target_pairs={{0,4},{4,0},{8,12},{12,8},{16,20},{20,16},{24,28},{28,24},{1,5},{5... | collective-permute-start | bytes 1179656 | tf_op jit(solution)/shard_map/ppermute | solution.py:431
  54.8 16.9 %collective-permute-start.27 = (bf16[256,768]{1,0:T(8,128)(2,1)S(1)}, bf16[256,768]{1,0:T(8,128)(2,1)S(1)}, u32[]{:S(2)}, u32[]{:S(2)}) collective-permute-start(bf16[256,768]{1,0:T(8,128)(2,1)S(1)} %copy-done.3), channel_id=1, source_target_pairs={{0,8},{4,12},{8,16},{12,20},{16,24},{20,28},{24,0},{28,4},{1,9},{5... | collective-permute-start | bytes 1179656 | tf_op jit(solution)/shard_map/ppermute | solution.py:427
  57.7 17.0 %collective-permute-start.14 = (bf16[256,768]{1,0:T(8,128)(2,1)S(1)}, bf16[256,768]{1,0:T(8,128)(2,1)S(1)}, u32[]{:S(2)}, u32[]{:S(2)}) collective-permute-start(bf16[256,768]{1,0:T(8,128)(2,1)S(1)} %collective-permute-done.13.refs_8_), channel_id=1, source_target_pairs={{0,4},{4,0},{8,12},{12,8},{16,20},{20,16},{24,28},{28,24},{1,5},{5... | collective-permute-start | bytes 1179656 | tf_op jit(solution)/shard_map/ppermute | solution.py:431
  63.2 10.4 %copy-start.15 = (bf16[256,768]{1,0:T(8,128)(2,1)}, bf16[256,768]{1,0:T(8,128)(2,1)S(1)}, u32[]{:S(2)}) copy-start(bf16[256,768]{1,0:T(8,128)(2,1)S(1)} %collective-permute-done.20.refs_2_) | copy-start | bytes 1179652
  63.2 17.0 %collective-permute-start.15 = (bf16[256,768]{1,0:T(8,128)(2,1)S(1)}, bf16[256,768]{1,0:T(8,128)(2,1)}, u32[]{:S(2)}, u32[]{:S(2)}) collective-permute-start(bf16[256,768]{1,0:T(8,128)(2,1)S(1)} %collective-permute-done.13.refs_8_), channel_id=1, source_target_pairs={{0,8},{4,12},{8,16},{12,20},{16,24},{20,28},{24,0},{28,4},{1,9},{5... | collective-permute-start | bytes 1179656 | tf_op jit(solution)/shard_map/ppermute | solution.py:427
  65.4 16.3 %collective-permute-start.21 = (bf16[256,768]{1,0:T(8,128)(2,1)S(1)}, bf16[256,768]{1,0:T(8,128)(2,1)S(1)}, u32[]{:S(2)}, u32[]{:S(2)}) collective-permute-start(bf16[256,768]{1,0:T(8,128)(2,1)S(1)} %collective-permute-done.20.refs_2_), channel_id=1, source_target_pairs={{0,4},{4,0},{8,12},{12,8},{16,20},{20,16},{24,28},{28,24},{1,5},{5... | collective-permute-start | bytes 1179656 | tf_op jit(solution)/shard_map/ppermute | solution.py:431
  71.6 17.0 %collective-permute-start.22 = (bf16[256,768]{1,0:T(8,128)(2,1)S(1)}, bf16[256,768]{1,0:T(8,128)(2,1)}, u32[]{:S(2)}, u32[]{:S(2)}) collective-permute-start(bf16[256,768]{1,0:T(8,128)(2,1)S(1)} %collective-permute-done.20.refs_2_), channel_id=1, source_target_pairs={{0,8},{4,12},{8,16},{12,20},{16,24},{20,28},{24,0},{28,4},{1,9},{5... | collective-permute-start | bytes 1179656 | tf_op jit(solution)/shard_map/ppermute | solution.py:427
  71.6 25.3 %collective-permute-start.28 = (bf16[256,768]{1,0:T(8,128)(2,1)S(1)}, bf16[256,768]{1,0:T(8,128)(2,1)S(1)}, u32[]{:S(2)}, u32[]{:S(2)}) collective-permute-start(bf16[256,768]{1,0:T(8,128)(2,1)S(1)} %collective-permute-done.27.refs_2_), channel_id=1, source_target_pairs={{0,8},{4,12},{8,16},{12,20},{16,24},{20,28},{24,0},{28,4},{1,9},{5... | collective-permute-start | bytes 1179656 | tf_op jit(solution)/shard_map/ppermute | solution.py:427
  75.5 39.9 %collective-permute-start.7 = (bf16[128,2048]{1,0:T(8,128)(2,1)S(1)}, bf16[128,2048]{1,0:T(8,128)(2,1)S(1)}, u32[]{:S(2)}, u32[]{:S(2)}) collective-permute-start(bf16[128,2048]{1,0:T(8,128)(2,1)S(1)} %get-tuple-element.40.refs_2_), channel_id=1, source_target_pairs={{0,1},{1,0},{2,3},{3,2},{4,5},{5,4},{6,7},{7,6},{8,9},{9,8},{10,11... | collective-permute-start | bytes 1572872 | tf_op jit(solution)/shard_map/ppermute | solution.py:420
  80.2 35.7 %collective-permute-start.10 = (bf16[128,2048]{1,0:T(8,128)(2,1)S(1)}, bf16[128,2048]{1,0:T(8,128)(2,1)S(1)}, u32[]{:S(2)}, u32[]{:S(2)}) collective-permute-start(bf16[128,2048]{1,0:T(8,128)(2,1)S(1)} %get-tuple-element.40.refs_2_), channel_id=1, source_target_pairs={{0,2},{1,3},{2,0},{3,1},{4,6},{5,7},{6,4},{7,5},{8,10},{9,11},{10,... | collective-permute-start | bytes 1572872 | tf_op jit(solution)/shard_map/ppermute | solution.py:421
  82.4 15.2 %collective-permute-start.16 = (bf16[256,768]{1,0:T(8,128)(2,1)}, bf16[256,768]{1,0:T(8,128)(2,1)}, u32[]{:S(2)}, u32[]{:S(2)}) collective-permute-start(bf16[256,768]{1,0:T(8,128)(2,1)} %collective-permute-done.15.refs_10_), channel_id=1, source_target_pairs={{0,4},{4,0},{8,12},{12,8},{16,20},{20,16},{24,28},{28,24},{1,5},{5... | collective-permute-start | bytes 1179656 | tf_op jit(solution)/shard_map/ppermute | solution.py:431
  88.6 16.9 %collective-permute-start.17 = (bf16[256,768]{1,0:T(8,128)(2,1)}, bf16[256,768]{1,0:T(8,128)(2,1)}, u32[]{:S(2)}, u32[]{:S(2)}) collective-permute-start(bf16[256,768]{1,0:T(8,128)(2,1)} %collective-permute-done.15.refs_10_), channel_id=1, source_target_pairs={{0,8},{4,12},{8,16},{12,20},{16,24},{20,28},{24,0},{28,4},{1,9},{5... | collective-permute-start | bytes 1179656 | tf_op jit(solution)/shard_map/ppermute | solution.py:427
  97.7 16.2 %collective-permute-start.24 = (bf16[256,768]{1,0:T(8,128)(2,1)}, bf16[256,768]{1,0:T(8,128)(2,1)}, u32[]{:S(2)}, u32[]{:S(2)}) collective-permute-start(bf16[256,768]{1,0:T(8,128)(2,1)} %collective-permute-done.22.refs_4_), channel_id=1, source_target_pairs={{0,8},{4,12},{8,16},{12,20},{16,24},{20,28},{24,0},{28,4},{1,9},{5... | collective-permute-start | bytes 1179656 | tf_op jit(solution)/shard_map/ppermute | solution.py:427
  97.7 47.2 %collective-permute-start.23 = (bf16[256,768]{1,0:T(8,128)(2,1)}, bf16[256,768]{1,0:T(8,128)(2,1)S(1)}, u32[]{:S(2)}, u32[]{:S(2)}) collective-permute-start(bf16[256,768]{1,0:T(8,128)(2,1)} %collective-permute-done.22.refs_4_), channel_id=1, source_target_pairs={{0,4},{4,0},{8,12},{12,8},{16,20},{20,16},{24,28},{28,24},{1,5},{5... | collective-permute-start | bytes 1179656 | tf_op jit(solution)/shard_map/ppermute | solution.py:431
  105.4 16.5 %collective-permute-start.32 = (bf16[256,768]{1,0:T(8,128)(2,1)}, bf16[256,768]{1,0:T(8,128)(2,1)S(1)}, u32[]{:S(2)}, u32[]{:S(2)}) collective-permute-start(bf16[256,768]{1,0:T(8,128)(2,1)} %copy-done.4), channel_id=1, source_target_pairs={{0,8},{4,12},{8,16},{12,20},{16,24},{20,28},{24,0},{28,4},{1,9},{5... | collective-permute-start | bytes 1179656 | tf_op jit(solution)/shard_map/ppermute | solution.py:427
  113.9 12.2 %collective-permute-start.18 = (bf16[256,768]{1,0:T(8,128)(2,1)}, bf16[256,768]{1,0:T(8,128)(2,1)S(1)}, u32[]{:S(2)}, u32[]{:S(2)}) collective-permute-start(bf16[256,768]{1,0:T(8,128)(2,1)} %collective-permute-done.17.refs_12_), channel_id=1, source_target_pairs={{0,4},{4,0},{8,12},{12,8},{16,20},{20,16},{24,28},{28,24},{1,5},{5... | collective-permute-start | bytes 1179656 | tf_op jit(solution)/shard_map/ppermute | solution.py:431
  115.4 29.6 %collective-permute-start.25 = (bf16[256,768]{1,0:T(8,128)(2,1)}, bf16[256,768]{1,0:T(8,128)(2,1)S(1)}, u32[]{:S(2)}, u32[]{:S(2)}) collective-permute-start(bf16[256,768]{1,0:T(8,128)(2,1)} %collective-permute-done.24.refs_6_), channel_id=1, source_target_pairs={{0,4},{4,0},{8,12},{12,8},{16,20},{20,16},{24,28},{28,24},{1,5},{5... | collective-permute-start | bytes 1179656 | tf_op jit(solution)/shard_map/ppermute | solution.py:431
  115.9 21.8 %collective-permute-start.11 = (bf16[128,2048]{1,0:T(8,128)(2,1)S(1)}, bf16[128,2048]{1,0:T(8,128)(2,1)S(1)}, u32[]{:S(2)}, u32[]{:S(2)}) collective-permute-start(bf16[128,2048]{1,0:T(8,128)(2,1)S(1)} %collective-permute-done.10.refs_4_), channel_id=1, source_target_pairs={{0,1},{1,0},{2,3},{3,2},{4,5},{5,4},{6,7},{7,6},{8,9},{9,8},{10,11... | collective-permute-start | bytes 1572872 | tf_op jit(solution)/shard_map/ppermute | solution.py:420
  115.9 29.0 %copy-start.25 = (f32[3,768]{1,0:T(4,128)S(1)}, f32[3,768]{1,0:T(4,128)}, u32[]{:S(2)}) copy-start(f32[3,768]{1,0:T(4,128)} %gate_taps.1) | copy-start | bytes 27652
  115.9 29.0 %copy-start.26 = (f32[3,768]{1,0:T(4,128)S(1)}, f32[3,768]{1,0:T(4,128)}, u32[]{:S(2)}) copy-start(f32[3,768]{1,0:T(4,128)} %value_taps.1) | copy-start | bytes 27652
  115.9 29.0 %copy-start.12 = (bf16[256,768]{1,0:T(8,128)(2,1)S(1)}, bf16[256,768]{1,0:T(8,128)(2,1)}, u32[]{:S(2)}) copy-start(bf16[256,768]{1,0:T(8,128)(2,1)} %refs_0_.3) | copy-start | bytes 1179652
  116.0 29.0 %copy-start.14 = (bf16[256,768]{1,0:T(8,128)(2,1)S(1)}, bf16[256,768]{1,0:T(8,128)(2,1)}, u32[]{:S(2)}) copy-start(bf16[256,768]{1,0:T(8,128)(2,1)} %copy-done.13) | copy-start | bytes 1179652
  116.0 29.0 %copy-start.16 = (bf16[256,768]{1,0:T(8,128)(2,1)S(1)}, bf16[256,768]{1,0:T(8,128)(2,1)}, u32[]{:S(2)}) copy-start(bf16[256,768]{1,0:T(8,128)(2,1)} %copy-done.15) | copy-start | bytes 1179652
  116.0 29.0 %copy-start.18 = (bf16[256,768]{1,0:T(8,128)(2,1)S(1)}, bf16[256,768]{1,0:T(8,128)(2,1)}, u32[]{:S(2)}) copy-start(bf16[256,768]{1,0:T(8,128)(2,1)} %copy-done.17) | copy-start | bytes 1179652
  121.9 4.8 %collective-permute-start.8 = (bf16[16,2048]{1,0:T(8,128)(2,1)S(1)}, bf16[16,2048]{1,0:T(8,128)(2,1)S(1)}, u32[]{:S(2)}, u32[]{:S(2)}) collective-permute-start(bf16[16,2048]{1,0:T(8,128)(2,1)S(1)} %slice_select_fusion), channel_id=1, source_target_pairs={{2,4},{3,5},{6,8},{7,9},{10,12},{11,13},{14,16},{15,17},{18,20},{1... | collective-permute-start | bytes 196616 | tf_op jit(solution)/shard_map/ppermute | solution.py:501
  126.1 3.3 %collective-permute-start.9 = (bf16[16,2048]{1,0:T(8,128)(2,1)S(1)}, bf16[16,2048]{1,0:T(8,128)(2,1)S(1)}, u32[]{:S(2)}, u32[]{:S(2)}) collective-permute-start(bf16[16,2048]{1,0:T(8,128)(2,1)S(1)} %slice_select_fusion), channel_id=1, source_target_pairs={{2,6},{3,7},{6,10},{7,11},{10,14},{11,15},{14,18},{15,19},{18,22},... | collective-permute-start | bytes 196616 | tf_op jit(solution)/shard_map/ppermute | solution.py:501
  126.7 25.2 %collective-permute-start.34 = (bf16[256,768]{1,0:T(8,128)(2,1)S(1)}, bf16[256,768]{1,0:T(8,128)(2,1)S(1)}, u32[]{:S(2)}, u32[]{:S(2)}) collective-permute-start(bf16[256,768]{1,0:T(8,128)(2,1)S(1)} %collective-permute-done.26.refs_1_), channel_id=1, source_target_pairs={{0,8},{4,12},{8,16},{12,20},{16,24},{20,28},{24,0},{28,4},{1,9},{5... | collective-permute-start | bytes 1179656 | tf_op jit(solution)/shard_map/ppermute | solution.py:429
  129.4 22.6 %collective-permute-start.33 = (bf16[256,768]{1,0:T(8,128)(2,1)}, bf16[256,768]{1,0:T(8,128)(2,1)S(1)}, u32[]{:S(2)}, u32[]{:S(2)}) collective-permute-start(bf16[256,768]{1,0:T(8,128)(2,1)} %copy-done.4), channel_id=1, source_target_pairs={{0,4},{4,0},{8,12},{12,8},{16,20},{20,16},{24,28},{28,24},{1,5},{5... | collective-permute-start | bytes 1179656 | tf_op jit(solution)/shard_map/ppermute | solution.py:431
  137.7 19.0 %collective-permute-start.38 = (bf16[256,768]{1,0:T(8,128)(2,1)S(1)}, bf16[256,768]{1,0:T(8,128)(2,1)S(1)}, u32[]{:S(2)}, u32[]{:S(2)}) collective-permute-start(bf16[256,768]{1,0:T(8,128)(2,1)S(1)} %collective-permute-done.32.refs_0_), channel_id=1, source_target_pairs={{0,4},{4,0},{8,12},{12,8},{16,20},{20,16},{24,28},{28,24},{1,5},{5... | collective-permute-start | bytes 1179656 | tf_op jit(solution)/shard_map/ppermute | solution.py:431
  145.0 5.7 %copy-start.5 = (bf16[256,768]{1,0:T(8,128)(2,1)S(1)}, bf16[256,768]{1,0:T(8,128)(2,1)}, u32[]{:S(2)}) copy-start(bf16[256,768]{1,0:T(8,128)(2,1)} %copy-done.4) | copy-start | bytes 1179652
  151.9 2.9 %collective-permute-start.29 = (bf16[128,1024]{1,0:T(8,128)(2,1)S(1)}, bf16[128,1024]{1,0:T(8,128)(2,1)S(1)}, u32[]{:S(2)}, u32[]{:S(2)}) collective-permute-start(bf16[128,1024]{1,0:T(8,128)(2,1)S(1)} %get-tuple-element.46), channel_id=1, source_target_pairs={{0,1},{1,0},{2,3},{3,2},{4,5},{5,4},{6,7},{7,6},{8,9},{9,8},{10,11... | collective-permute-start | bytes 786440 | tf_op jit(solution)/shard_map/ppermute | solution.py:420
  153.0 6.2 %collective-permute-start.35 = (bf16[128,768]{1,0:T(8,128)(2,1)S(1)}, bf16[128,768]{1,0:T(8,128)(2,1)S(1)}, u32[]{:S(2)}, u32[]{:S(2)}) collective-permute-start(bf16[128,768]{1,0:T(8,128)(2,1)S(1)} %get-tuple-element.50), channel_id=1, source_target_pairs={{0,1},{1,0},{2,3},{3,2},{4,5},{5,4},{6,7},{7,6},{8,9},{9,8},{10,11... | collective-permute-start | bytes 589832 | tf_op jit(solution)/shard_map/ppermute | solution.py:420
  154.7 15.1 %collective-permute-start.31 = (bf16[128,1024]{1,0:T(8,128)(2,1)S(1)}, bf16[128,1024]{1,0:T(8,128)(2,1)S(1)}, u32[]{:S(2)}, u32[]{:S(2)}) collective-permute-start(bf16[128,1024]{1,0:T(8,128)(2,1)S(1)} %get-tuple-element.48), channel_id=1, source_target_pairs={{0,1},{1,0},{2,3},{3,2},{4,5},{5,4},{6,7},{7,6},{8,9},{9,8},{10,11... | collective-permute-start | bytes 786440 | tf_op jit(solution)/shard_map/ppermute | solution.py:420
  155.4 14.4 %collective-permute-start.30 = (bf16[128,1024]{1,0:T(8,128)(2,1)S(1)}, bf16[128,1024]{1,0:T(8,128)(2,1)S(1)}, u32[]{:S(2)}, u32[]{:S(2)}) collective-permute-start(bf16[128,1024]{1,0:T(8,128)(2,1)S(1)} %shard_map.166), channel_id=1, source_target_pairs={{0,2},{1,3},{2,0},{3,1},{4,6},{5,7},{6,4},{7,5},{8,10},{9,11},{10,... | collective-permute-start | bytes 786440 | tf_op jit(solution)/shard_map/ppermute | solution.py:543
  157.5 12.3 %copy-start.29 = (f32[2048]{0:T(1024)S(1)}, f32[2048]{0:T(1024)}, u32[]{:S(2)}) copy-start(f32[2048]{0:T(1024)} %param.31) | copy-start | bytes 24580
  157.6 4.0 %collective-permute-start.39 = (bf16[128,256]{1,0:T(8,128)(2,1)S(1)}, bf16[128,256]{1,0:T(8,128)(2,1)S(1)}, u32[]{:S(2)}, u32[]{:S(2)}) collective-permute-start(bf16[128,256]{1,0:T(8,128)(2,1)S(1)} %get-tuple-element.54), channel_id=1, source_target_pairs={{0,1},{1,0},{2,3},{3,2},{4,5},{5,4},{6,7},{7,6},{8,9},{9,8},{10,11... | collective-permute-start | bytes 196616 | tf_op jit(solution)/shard_map/ppermute | solution.py:420
  158.9 10.9 %collective-permute-start.37 = (bf16[128,768]{1,0:T(8,128)(2,1)S(1)}, bf16[128,768]{1,0:T(8,128)(2,1)S(1)}, u32[]{:S(2)}, u32[]{:S(2)}) collective-permute-start(bf16[128,768]{1,0:T(8,128)(2,1)S(1)} %get-tuple-element.52), channel_id=1, source_target_pairs={{0,1},{1,0},{2,3},{3,2},{4,5},{5,4},{6,7},{7,6},{8,9},{9,8},{10,11... | collective-permute-start | bytes 589832 | tf_op jit(solution)/shard_map/ppermute | solution.py:420
  159.8 10.0 %collective-permute-start.36 = (bf16[128,768]{1,0:T(8,128)(2,1)S(1)}, bf16[128,768]{1,0:T(8,128)(2,1)S(1)}, u32[]{:S(2)}, u32[]{:S(2)}) collective-permute-start(bf16[128,768]{1,0:T(8,128)(2,1)S(1)} %shard_map.169), channel_id=1, source_target_pairs={{0,2},{1,3},{2,0},{3,1},{4,6},{5,7},{6,4},{7,5},{8,10},{9,11},{10,... | collective-permute-start | bytes 589832 | tf_op jit(solution)/shard_map/ppermute | solution.py:543
  161.6 1.3 collective-permute-start.41
  162.9 6.9 %collective-permute-start.40 = (bf16[128,256]{1,0:T(8,128)(2,1)S(1)}, bf16[128,256]{1,0:T(8,128)(2,1)S(1)}, u32[]{:S(2)}, u32[]{:S(2)}) collective-permute-start(bf16[128,256]{1,0:T(8,128)(2,1)S(1)} %shard_map.172), channel_id=1, source_target_pairs={{0,2},{1,3},{2,0},{3,1},{4,6},{5,7},{6,4},{7,5},{8,10},{9,11},{10,... | collective-permute-start | bytes 196616 | tf_op jit(solution)/shard_map/ppermute | solution.py:543
  (13 other events, 10.9 us)

commit v2 on v1

--- a/solution.py
+++ b/solution.py
@@ -358,11 +358,10 @@
     out[...] = (mine[...].astype(f32) + theirs[...].astype(f32)).astype(bf16)
 
 
-def result_kernel(groups, rows, nz, pair, info, stream, post_gain, *refs):
+def result_kernel(groups, counts, rows, nz, pair, info, stream, post_gain, *refs):
     out, summed = refs[-2], refs[-1]
-    count = (len(refs) - 2) // len(groups)
     for g, order in enumerate(groups):
-        parts = refs[g * count : (g + 1) * count]
+        parts = refs[sum(counts[:g]) : sum(counts[: g + 1])]
         total = parts[0][...].astype(f32)
         for part in parts[1:]:
             total = total + part[...].astype(f32)
@@ -536,15 +535,22 @@
                 (shape, shape),
                 (info, hidden_keep, hidden_send, *(downs[o] for o in blocks)),
             )
+            straight = [(i, (i + 2 * d) % n_tp) for i in range(n_tp)]
+            crossed = [(i, ((i + 2 * d) % n_tp) ^ 1) for i in range(n_tp)]
+            if d and g and g == len(groups) - 1:
+                parts[g].append(lax.ppermute(mine, "tp", straight))
+                parts[g].append(lax.ppermute(away, "tp", crossed))
+                continue
             theirs = mate(away)
             if d:
                 both = call(add_kernel, shape, (info, mine, theirs))
-                route = [(i, (i + 2 * d) % n_tp) for i in range(n_tp)]
-                parts[g].append(lax.ppermute(both, "tp", route))
+                parts[g].append(lax.ppermute(both, "tp", straight))
             else:
                 parts[g] += [mine, theirs]
     return call(
-        functools.partial(result_kernel, groups, rows_of, wide, paired),
+        functools.partial(
+            result_kernel, groups, [len(p) for p in parts], rows_of, wide, paired
+        ),
         ((step, model), bf16),
         (info, stream, post_gain[None], *(p for group in parts for p in group)),
         scratch=(pltpu.VMEM((step, model), f32),),

time: 172 us -> 174 us (1.012)
  waiting for transfers between devices: 78.9 us -> 81.9 us
    ppermute x3 -> x4, waiting for transfers between devices: 5.7 us -> 8.42 us  [the longest x1 4.63 us: layer(): parts[g].append(lax.ppermute(mine, 'tp', straight))]
    pallas_call x21 -> x20, Pallas kernels: 30.5 us -> 29.9 us  [call(): pl.pallas_call(kernel, out_shape=tuple((jax.ShapeDtypeStruct(*o) for o in...]
  transfers between devices with their start and end apart: 42 -> 42, of which waited for: 18 -> 19; matrix products, arithmetic and copies ran while one was open for 0% -> 0% of each run, Pallas kernels for 17% -> 16%
where the time goes in v2:
time: 174 us
  waiting for transfers between devices  81.9 us (47%)
  starting transfers between devices  50.6 us (29%)
  Pallas kernels  29.9 us (17%)
  local copies, waits for them, and re-layouts  11 us (6%)
    ppermute x9, waiting for transfers between devices, spread(): found[k, 0] = lax.ppermute(found[k - 1, 0], 'sp', ring)  52.8 us
    pallas_call x20, Pallas kernels, call(): pl.pallas_call(kernel, out_shape=tuple((jax.ShapeDtypeStruct(*o) for o in...  29.9 us
    ppermute x11, starting transfers between devices, spread(): found[k, 1] = lax.ppermute(found[k, 0], 'sp', swap)  19 us
    unnamed x70, local copies, waits for them, and re-layouts  11 us
    ppermute x2, starting transfers between devices, layer(): states.insert(0, lax.ppermute(total, 'sp', route))  9.28 us
    ppermute x11, waiting for transfers between devices, spread(): found[k, 1] = lax.ppermute(found[k, 0], 'sp', swap)  6.98 us
    ppermute x9, starting transfers between devices, spread(): found[k, 0] = lax.ppermute(found[k - 1, 0], 'sp', ring)  6.09 us
    ppermute x2, waiting for transfers between devices, layer(): states.insert(0, lax.ppermute(total, 'sp', route))  5.52 us
  transfers between devices with their start and end apart: 42, of which 19 were waited for; matrix products, arithmetic and copies ran while one was open for 0% of the time, Pallas kernels for 16%

profile of v2, /device:TPU:0, one launch (start us, length us, event | category | flops | bytes accessed | tf_op | source)
XLA Modules:
  0.0 174.0 jit_solution(333655454366779340)
XLA Ops:
  0.5 1.0 copy-done.1
  1.5 0.9 copy-done.6
  3.9 1.8 %shard_map.155 = (bf16[1,144,512]{2,1,0:T(8,128)(2,1)S(1)}, bf16[1,144,512]{2,1,0:T(8,128)(2,1)S(1)}) custom-call(s32[8]{0:T(128)S(1)} %compare_select_fusion.2.info, bf16[512,256]{1,0:T(8,128)(2,1)S(1)} %copy-done.6, bf16[512,512]{1,0:T(8,128)(2,1)S(1)} %copy-done.1, f32[1,512]{1,0:T(1,128)S(1)} %copy-done.30, f32[1,512]{1,0:T(1,128)S(1)} %copy-done.32), custom_call_target="tpu_custom_call" | custom-call | tf_op jit(solution)/shard_map/pallas_call | solution.py:33
  5.7 2.6 %collective-permute-start = (bf16[1,144,512]{2,1,0:T(8,128)(2,1)S(1)}, bf16[1,144,512]{2,1,0:T(8,128)(2,1)S(1)}, u32[]{:S(2)}, u32[]{:S(2)}) collective-permute-start(bf16[1,144,512]{2,1,0:T(8,128)(2,1)S(1)} %get-tuple-element.34), channel_id=1, source_target_pairs={{0,4},{4,0},{8,12},{12,8},{16,20},{20,16},{24,28},{28,24},{1,5},{5... | collective-permute-start | bytes 442376 | tf_op jit(solution)/shard_map/ppermute | solution.py:456
  8.3 4.5 %collective-permute-done.theirs = bf16[1,144,512]{2,1,0:T(8,128)(2,1)S(1)} collective-permute-done((bf16[1,144,512]{2,1,0:T(8,128)(2,1)S(1)}, bf16[1,144,512]{2,1,0:T(8,128)(2,1)S(1)}, u32[]{:S(2)}, u32[]{:S(2)}) %collective-permute-start) | collective-permute-done | bytes 147488 | tf_op jit(solution)/shard_map/ppermute | solution.py:456
  13.4 3.7 %collective-permute-start.1 = (bf16[1,144,512]{2,1,0:T(8,128)(2,1)S(1)}, bf16[1,144,512]{2,1,0:T(8,128)(2,1)S(1)}, u32[]{:S(2)}, u32[]{:S(2)}) collective-permute-start(bf16[1,144,512]{2,1,0:T(8,128)(2,1)S(1)} %shard_map.156.later), channel_id=1, source_target_pairs={{0,8},{4,12},{8,16},{12,20},{16,24},{20,28},{1,9},{5,13},{9,17},{1... | collective-permute-start | bytes 442376 | tf_op jit(solution)/shard_map/ppermute | solution.py:462
  17.2 2.8 %collective-permute-done.1.earlier.refs_1_ = bf16[1,144,512]{2,1,0:T(8,128)(2,1)S(1)} collective-permute-done((bf16[1,144,512]{2,1,0:T(8,128)(2,1)S(1)}, bf16[1,144,512]{2,1,0:T(8,128)(2,1)S(1)}, u32[]{:S(2)}, u32[]{:S(2)}) %collective-permute-start.1) | collective-permute-done | bytes 147488 | tf_op jit(solution)/shard_map/ppermute | solution.py:462
  20.7 5.5 %collective-permute-start.2 = (bf16[1,144,512]{2,1,0:T(8,128)(2,1)S(1)}, bf16[1,144,512]{2,1,0:T(8,128)(2,1)S(1)}, u32[]{:S(2)}, u32[]{:S(2)}) collective-permute-start(bf16[1,144,512]{2,1,0:T(8,128)(2,1)S(1)} %shard_map.157), channel_id=1, source_target_pairs={{0,16},{4,20},{8,24},{12,28},{1,17},{5,21},{9,25},{13,29},{2,18},{... | collective-permute-start | bytes 442376 | tf_op jit(solution)/shard_map/ppermute | solution.py:462
  26.3 2.7 %collective-permute-done.2.refs_0_ = bf16[1,144,512]{2,1,0:T(8,128)(2,1)S(1)} collective-permute-done((bf16[1,144,512]{2,1,0:T(8,128)(2,1)S(1)}, bf16[1,144,512]{2,1,0:T(8,128)(2,1)S(1)}, u32[]{:S(2)}, u32[]{:S(2)}) %collective-permute-start.2) | collective-permute-done | bytes 147488 | tf_op jit(solution)/shard_map/ppermute | solution.py:462
  28.9 0.8 shard_map.158
  29.7 1.6 collective-permute-start.3
  31.8 1.9 %shard_map.154 = (f32[512,512]{1,0:T(8,128)S(1)}, f32[1,512,128]{2,1,0:T(8,128)S(1)}) custom-call(s32[8]{0:T(128)S(1)} %compare_select_fusion.2.info, bf16[512,256]{1,0:T(8,128)(2,1)S(1)} %copy-done.8, bf16[512,256]{1,0:T(8,128)(2,1)S(1)} %copy-done.7, bf16[512,512]{1,0:T(8,128)(2,1)S(1)} %copy-done.2, f32[1,512]{1,0:T(1,128)S(1)} %copy-done.31, ...), custom_call_target="tpu_custom_call" | custom-call | tf_op jit(solution)/shard_map/pallas_call | solution.py:33
  33.7 2.8 %collective-permute-done.3.theirs = bf16[1,144,512]{2,1,0:T(8,128)(2,1)S(1)} collective-permute-done((bf16[1,144,512]{2,1,0:T(8,128)(2,1)S(1)}, bf16[1,144,512]{2,1,0:T(8,128)(2,1)S(1)}, u32[]{:S(2)}, u32[]{:S(2)}) %collective-permute-start.3) | collective-permute-done | bytes 147488 | tf_op jit(solution)/shard_map/ppermute | solution.py:467
  36.5 1.4 shard_map.159
  38.0 4.0 %collective-permute-start.13 = (bf16[256,768]{1,0:T(8,128)(2,1)S(1)}, bf16[256,768]{1,0:T(8,128)(2,1)S(1)}, u32[]{:S(2)}, u32[]{:S(2)}) collective-permute-start(bf16[256,768]{1,0:T(8,128)(2,1)S(1)} %copy-done.34), channel_id=1, source_target_pairs={{0,8},{4,12},{8,16},{12,20},{16,24},{20,28},{24,0},{28,4},{1,9},{5... | collective-permute-start | bytes 1179656 | tf_op jit(solution)/shard_map/ppermute | solution.py:426
  42.0 1.3 shard_map.160
  43.3 1.6 collective-permute-start.6
  44.9 1.5 collective-permute-start.19
  46.4 1.4 collective-permute-start.20
  47.9 0.7 copy-done.19
  49.2 5.6 %collective-permute-done.13.refs_8_ = bf16[256,768]{1,0:T(8,128)(2,1)S(1)} collective-permute-done((bf16[256,768]{1,0:T(8,128)(2,1)S(1)}, bf16[256,768]{1,0:T(8,128)(2,1)S(1)}, u32[]{:S(2)}, u32[]{:S(2)}) %collective-permute-start.13) | collective-permute-done | bytes 393248 | tf_op jit(solution)/shard_map/ppermute | solution.py:426
  54.8 2.1 %collective-permute-done.19.refs_1_ = bf16[256,768]{1,0:T(8,128)(2,1)S(1)} collective-permute-done((bf16[256,768]{1,0:T(8,128)(2,1)S(1)}, bf16[256,768]{1,0:T(8,128)(2,1)S(1)}, u32[]{:S(2)}, u32[]{:S(2)}) %collective-permute-start.19) | collective-permute-done | bytes 393248 | tf_op jit(solution)/shard_map/ppermute | solution.py:430
  56.9 0.7 copy-done.13
  57.7 1.5 collective-permute-start.14
  59.2 4.0 %collective-permute-done.20.refs_2_ = bf16[256,768]{1,0:T(8,128)(2,1)S(1)} collective-permute-done((bf16[256,768]{1,0:T(8,128)(2,1)S(1)}, bf16[256,768]{1,0:T(8,128)(2,1)S(1)}, u32[]{:S(2)}, u32[]{:S(2)}) %collective-permute-start.20) | collective-permute-done | bytes 393248 | tf_op jit(solution)/shard_map/ppermute | solution.py:426
  63.2 0.8 copy-done.21
  64.0 1.4 collective-permute-done.26.refs_1_
  65.4 1.5 collective-permute-start.21
  66.8 4.8 %collective-permute-done.27.refs_2_ = bf16[256,768]{1,0:T(8,128)(2,1)S(1)} collective-permute-done((bf16[256,768]{1,0:T(8,128)(2,1)S(1)}, bf16[256,768]{1,0:T(8,128)(2,1)S(1)}, u32[]{:S(2)}, u32[]{:S(2)}) %collective-permute-start.27) | collective-permute-done | bytes 393248 | tf_op jit(solution)/shard_map/ppermute | solution.py:426
  72.3 1.3 shard_map.161.refs_1_
  73.6 1.1 shard_map.162
  75.5 4.7 %collective-permute-done.15.refs_10_ = bf16[256,768]{1,0:T(8,128)(2,1)} collective-permute-done((bf16[256,768]{1,0:T(8,128)(2,1)S(1)}, bf16[256,768]{1,0:T(8,128)(2,1)}, u32[]{:S(2)}, u32[]{:S(2)}) %collective-permute-start.15) | collective-permute-done | bytes 393248 | tf_op jit(solution)/shard_map/ppermute | solution.py:426
  80.2 1.5 collective-permute-start.10
  81.7 0.8 copy-done.17
  82.4 1.5 collective-permute-start.16
  83.9 4.7 %collective-permute-done.22.refs_4_ = bf16[256,768]{1,0:T(8,128)(2,1)} collective-permute-done((bf16[256,768]{1,0:T(8,128)(2,1)S(1)}, bf16[256,768]{1,0:T(8,128)(2,1)}, u32[]{:S(2)}, u32[]{:S(2)}) %collective-permute-start.22) | collective-permute-done | bytes 393248 | tf_op jit(solution)/shard_map/ppermute | solution.py:426
  88.6 8.3 %collective-permute-done.28.refs_3_ = bf16[256,768]{1,0:T(8,128)(2,1)S(1)} collective-permute-done((bf16[256,768]{1,0:T(8,128)(2,1)S(1)}, bf16[256,768]{1,0:T(8,128)(2,1)S(1)}, u32[]{:S(2)}, u32[]{:S(2)}) %collective-permute-start.28) | collective-permute-done | bytes 393248 | tf_op jit(solution)/shard_map/ppermute | solution.py:426
  96.9 0.8 copy-done.4
  97.7 1.5 collective-permute-start.23
  99.2 6.3 %collective-permute-done.17.refs_12_ = bf16[256,768]{1,0:T(8,128)(2,1)} collective-permute-done((bf16[256,768]{1,0:T(8,128)(2,1)}, bf16[256,768]{1,0:T(8,128)(2,1)}, u32[]{:S(2)}, u32[]{:S(2)}) %collective-permute-start.17) | collective-permute-done | bytes 393248 | tf_op jit(solution)/shard_map/ppermute | solution.py:426
  105.4 8.4 %collective-permute-done.24.refs_6_ = bf16[256,768]{1,0:T(8,128)(2,1)} collective-permute-done((bf16[256,768]{1,0:T(8,128)(2,1)}, bf16[256,768]{1,0:T(8,128)(2,1)}, u32[]{:S(2)}, u32[]{:S(2)}) %collective-permute-start.24) | collective-permute-done | bytes 393248 | tf_op jit(solution)/shard_map/ppermute | solution.py:426
  113.9 1.5 collective-permute-start.18
  116.0 6.0 %collective-permute-done.32.refs_0_ = bf16[256,768]{1,0:T(8,128)(2,1)S(1)} collective-permute-done((bf16[256,768]{1,0:T(8,128)(2,1)}, bf16[256,768]{1,0:T(8,128)(2,1)S(1)}, u32[]{:S(2)}, u32[]{:S(2)}) %collective-permute-start.32) | collective-permute-done | bytes 393248 | tf_op jit(solution)/shard_map/ppermute | solution.py:426
  122.6 3.5 %collective-permute-done.18.refs_13_ = bf16[256,768]{1,0:T(8,128)(2,1)S(1)} collective-permute-done((bf16[256,768]{1,0:T(8,128)(2,1)}, bf16[256,768]{1,0:T(8,128)(2,1)S(1)}, u32[]{:S(2)}, u32[]{:S(2)}) %collective-permute-start.18) | collective-permute-done | bytes 393248 | tf_op jit(solution)/shard_map/ppermute | solution.py:430
  126.7 2.6 %collective-permute-start.34 = (bf16[256,768]{1,0:T(8,128)(2,1)S(1)}, bf16[256,768]{1,0:T(8,128)(2,1)S(1)}, u32[]{:S(2)}, u32[]{:S(2)}) collective-permute-start(bf16[256,768]{1,0:T(8,128)(2,1)S(1)} %collective-permute-done.26.refs_1_), channel_id=1, source_target_pairs={{0,8},{4,12},{8,16},{12,20},{16,24},{20,28},{24,0},{28,4},{1,9},{5... | collective-permute-start | bytes 1179656 | tf_op jit(solution)/shard_map/ppermute | solution.py:428
  129.4 8.3 %collective-permute-start.33 = (bf16[256,768]{1,0:T(8,128)(2,1)}, bf16[256,768]{1,0:T(8,128)(2,1)S(1)}, u32[]{:S(2)}, u32[]{:S(2)}) collective-permute-start(bf16[256,768]{1,0:T(8,128)(2,1)} %copy-done.4), channel_id=1, source_target_pairs={{0,4},{4,0},{8,12},{12,8},{16,20},{20,16},{24,28},{28,24},{1,5},{5... | collective-permute-start | bytes 1179656 | tf_op jit(solution)/shard_map/ppermute | solution.py:430
  137.8 1.0 copy-done.20
  138.8 1.0 copy-done.22
  139.8 1.0 copy-done.24
  140.8 4.1 %shard_map.163 = (bf16[528,768]{1,0:T(8,128)(2,1)S(1)}, bf16[528,2048]{1,0:T(8,128)(2,1)S(1)}) custom-call(s32[8]{0:T(128)S(1)} %compare_select_fusion.2.info, bf16[16,2048]{1,0:T(8,128)(2,1)S(1)} %collective-permute-done.8.refs_0_, bf16[16,2048]{1,0:T(8,128)(2,1)S(1)} %collective-permute-done.9.refs_1_, bf16[128,2048]{1,0:T(8,128)(2,1)S(1)} %get-tuple-element.40.refs_2_, ...), custom_call_target="tpu_custom_call" | custom-call | tf_op jit(solution)/shard_map/pallas_call | solution.py:33
  145.0 5.7 %shard_map.164 = (bf16[2,128,768]{2,1,0:T(8,128)(2,1)S(1)}, bf16[2,128,768]{2,1,0:T(8,128)(2,1)S(1)}) custom-call(s32[8]{0:T(128)S(1)} %compare_select_fusion.2.info, f32[3,768]{1,0:T(4,128)S(1)} %copy-done.25, f32[3,768]{1,0:T(4,128)S(1)} %copy-done.26, bf16[528,2048]{1,0:T(8,128)(2,1)S(1)} %get-tuple-element.41.rows_all, ...), custom_call_target="tpu_custom_call" | custom-call | tf_op jit(solution)/shard_map/pallas_call | solution.py:33
  150.7 1.1 shard_map.165
  152.0 1.0 shard_map.168
  153.6 1.1 shard_map.167
  155.4 1.3 collective-permute-start.30
  156.7 0.8 shard_map.171
  157.6 0.9 collective-permute-start.39
  158.4 1.0 shard_map.170
  160.2 1.3 collective-permute-start.36
  161.4 4.6 %collective-permute-done.39.refs_6_ = bf16[128,256]{1,0:T(8,128)(2,1)S(1)} collective-permute-done((bf16[128,256]{1,0:T(8,128)(2,1)S(1)}, bf16[128,256]{1,0:T(8,128)(2,1)S(1)}, u32[]{:S(2)}, u32[]{:S(2)}) %collective-permute-start.39) | collective-permute-done | bytes 65568 | tf_op jit(solution)/shard_map/ppermute | solution.py:541
  166.1 0.8 shard_map.172
  166.9 3.8 %collective-permute-done.40.refs_7_ = bf16[128,256]{1,0:T(8,128)(2,1)S(1)} collective-permute-done((bf16[128,256]{1,0:T(8,128)(2,1)S(1)}, bf16[128,256]{1,0:T(8,128)(2,1)S(1)}, u32[]{:S(2)}, u32[]{:S(2)}) %collective-permute-start.40) | collective-permute-done | bytes 65568 | tf_op jit(solution)/shard_map/ppermute | solution.py:542
  171.0 0.9 collective-permute-done.41.refs_9_
  172.0 2.0 %shard_map.173 = bf16[128,2048]{1,0:T(8,128)(2,1)} custom-call(s32[8]{0:T(128)S(1)} %compare_select_fusion.2.info, bf16[128,2048]{1,0:T(8,128)(2,1)S(1)} %get-tuple-element.39.stream, f32[1,2048]{1,0:T(1,128)S(1)} %bitcast.5, bf16[128,1024]{1,0:T(8,128)(2,1)S(1)} %collective-permute-done.30.refs_0_, bf16[128,1024]{1,0:T(8,128)(2,1)S(1)} %get-tuple-element.47.refs_1_, ...), custom_call_target="tpu_custom_call" | custom-call | tf_op jit(solution)/shard_map/pallas_call | solution.py:33
  (112 shorter events, 10.2 us)
Async XLA Ops:
  0.0 31.8 %copy-start.31 = (f32[1,512]{1,0:T(1,128)S(1)}, f32[1,512]{1,0:T(1,128)}, u32[]{:S(2)}) copy-start(f32[1,512]{1,0:T(1,128)} %ig.3) | copy-start | bytes 6148
  0.0 31.8 %copy-start.33 = (f32[1,512]{1,0:T(1,128)S(1)}, f32[1,512]{1,0:T(1,128)}, u32[]{:S(2)}) copy-start(f32[1,512]{1,0:T(1,128)} %fg.3) | copy-start | bytes 6148
  0.0 42.0 %collective-permute-start.5 = (bf16[512,2048]{1,0:T(8,128)(2,1)}, bf16[512,2048]{1,0:T(8,128)(2,1)S(1)}, u32[]{:S(2)}, u32[]{:S(2)}) collective-permute-start(bf16[512,2048]{1,0:T(8,128)(2,1)} %own_weight.3), channel_id=1, source_target_pairs={{0,1},{1,0},{2,3},{3,2},{4,5},{5,4},{6,7},{7,6},{8,9},{9,8},{10,11... | collective-permute-start | bytes 6291464 | tf_op jit(solution)/shard_map/ppermute | solution.py:419
  3.9 27.4 %copy-start.34 = (bf16[256,768]{1,0:T(8,128)(2,1)S(1)}, bf16[256,768]{1,0:T(8,128)(2,1)}, u32[]{:S(2)}) copy-start(bf16[256,768]{1,0:T(8,128)(2,1)} %refs_6_.1) | copy-start | bytes 1179652
  3.9 28.0 %copy-start.2 = (bf16[512,512]{1,0:T(8,128)(2,1)S(1)}, bf16[512,512]{1,0:T(8,128)(2,1)}, u32[]{:S(2)}) copy-start(bf16[512,512]{1,0:T(8,128)(2,1)} %value.3) | copy-start | bytes 1572868
  3.9 28.0 %copy-start.7 = (bf16[512,256]{1,0:T(8,128)(2,1)S(1)}, bf16[512,256]{1,0:T(8,128)(2,1)}, u32[]{:S(2)}) copy-start(bf16[512,256]{1,0:T(8,128)(2,1)} %key.3) | copy-start | bytes 786436
  3.9 28.0 %copy-start.8 = (bf16[512,256]{1,0:T(8,128)(2,1)S(1)}, bf16[512,256]{1,0:T(8,128)(2,1)}, u32[]{:S(2)}) copy-start(bf16[512,256]{1,0:T(8,128)(2,1)} %query.3) | copy-start | bytes 786436
  3.9 32.6 %copy-start.10 = (bf16[512,512]{1,0:T(8,128)(2,1)S(1)}, bf16[512,512]{1,0:T(8,128)(2,1)}, u32[]{:S(2)}) copy-start(bf16[512,512]{1,0:T(8,128)(2,1)} %out_gate.1) | copy-start | bytes 1572868
  5.7 7.1 %collective-permute-start = (bf16[1,144,512]{2,1,0:T(8,128)(2,1)S(1)}, bf16[1,144,512]{2,1,0:T(8,128)(2,1)S(1)}, u32[]{:S(2)}, u32[]{:S(2)}) collective-permute-start(bf16[1,144,512]{2,1,0:T(8,128)(2,1)S(1)} %get-tuple-element.34), channel_id=1, source_target_pairs={{0,4},{4,0},{8,12},{12,8},{16,20},{20,16},{24,28},{28,24},{1,5},{5... | collective-permute-start | bytes 442376 | tf_op jit(solution)/shard_map/ppermute | solution.py:456
  13.4 6.6 %collective-permute-start.1 = (bf16[1,144,512]{2,1,0:T(8,128)(2,1)S(1)}, bf16[1,144,512]{2,1,0:T(8,128)(2,1)S(1)}, u32[]{:S(2)}, u32[]{:S(2)}) collective-permute-start(bf16[1,144,512]{2,1,0:T(8,128)(2,1)S(1)} %shard_map.156.later), channel_id=1, source_target_pairs={{0,8},{4,12},{8,16},{12,20},{16,24},{20,28},{1,9},{5,13},{9,17},{1... | collective-permute-start | bytes 442376 | tf_op jit(solution)/shard_map/ppermute | solution.py:462
  20.7 21.3 %copy-start = (bf16[512,2048]{1,0:T(8,128)(2,1)S(1)}, bf16[512,2048]{1,0:T(8,128)(2,1)}, u32[]{:S(2)}) copy-start(bf16[512,2048]{1,0:T(8,128)(2,1)} %own_weight.3) | copy-start | bytes 6291460
  20.7 8.2 %collective-permute-start.2 = (bf16[1,144,512]{2,1,0:T(8,128)(2,1)S(1)}, bf16[1,144,512]{2,1,0:T(8,128)(2,1)S(1)}, u32[]{:S(2)}, u32[]{:S(2)}) collective-permute-start(bf16[1,144,512]{2,1,0:T(8,128)(2,1)S(1)} %shard_map.157), channel_id=1, source_target_pairs={{0,16},{4,20},{8,24},{12,28},{1,17},{5,21},{9,25},{13,29},{2,18},{... | collective-permute-start | bytes 442376 | tf_op jit(solution)/shard_map/ppermute | solution.py:462
  29.7 6.8 %collective-permute-start.3 = (bf16[1,144,512]{2,1,0:T(8,128)(2,1)S(1)}, bf16[1,144,512]{2,1,0:T(8,128)(2,1)S(1)}, u32[]{:S(2)}, u32[]{:S(2)}) collective-permute-start(bf16[1,144,512]{2,1,0:T(8,128)(2,1)S(1)} %get-tuple-element.36), channel_id=1, source_target_pairs={{0,4},{4,0},{8,12},{12,8},{16,20},{20,16},{24,28},{28,24},{1,5},{5... | collective-permute-start | bytes 442376 | tf_op jit(solution)/shard_map/ppermute | solution.py:467
  31.3 16.6 %collective-permute-start.12 = (bf16[256,768]{1,0:T(8,128)(2,1)S(1)}, bf16[256,768]{1,0:T(8,128)(2,1)S(1)}, u32[]{:S(2)}, u32[]{:S(2)}) collective-permute-start(bf16[256,768]{1,0:T(8,128)(2,1)S(1)} %copy-done.34), channel_id=1, source_target_pairs={{0,4},{4,0},{8,12},{12,8},{16,20},{20,16},{24,28},{28,24},{1,5},{5... | collective-permute-start | bytes 1179656 | tf_op jit(solution)/shard_map/ppermute | solution.py:430
  37.9 4.1 %collective-permute-start.4 = (bf16[2,128,512]{2,1,0:T(8,128)(2,1)S(1)}, bf16[2,128,512]{2,1,0:T(8,128)(2,1)S(1)}, u32[]{:S(2)}, u32[]{:S(2)}) collective-permute-start(bf16[2,128,512]{2,1,0:T(8,128)(2,1)S(1)} %get-tuple-element.38), channel_id=1, source_target_pairs={{0,1},{1,0},{2,3},{3,2},{4,5},{5,4},{6,7},{7,6},{8,9},{9,8},{10,11... | collective-permute-start | bytes 786440 | tf_op jit(solution)/shard_map/ppermute | solution.py:419
  38.0 16.8 %collective-permute-start.13 = (bf16[256,768]{1,0:T(8,128)(2,1)S(1)}, bf16[256,768]{1,0:T(8,128)(2,1)S(1)}, u32[]{:S(2)}, u32[]{:S(2)}) collective-permute-start(bf16[256,768]{1,0:T(8,128)(2,1)S(1)} %copy-done.34), channel_id=1, source_target_pairs={{0,8},{4,12},{8,16},{12,20},{16,24},{20,28},{24,0},{28,4},{1,9},{5... | collective-permute-start | bytes 1179656 | tf_op jit(solution)/shard_map/ppermute | solution.py:426
  42.0 2.9 %copy-start.11 = (bf16[256,768]{1,0:T(8,128)(2,1)S(1)}, bf16[256,768]{1,0:T(8,128)(2,1)}, u32[]{:S(2)}) copy-start(bf16[256,768]{1,0:T(8,128)(2,1)} %refs_0_.3) | copy-start | bytes 1179652
  42.0 6.6 %copy-start.3 = (bf16[256,768]{1,0:T(8,128)(2,1)S(1)}, bf16[256,768]{1,0:T(8,128)(2,1)}, u32[]{:S(2)}) copy-start(bf16[256,768]{1,0:T(8,128)(2,1)} %refs_0_.5) | copy-start | bytes 1179652
  43.3 30.3 %copy-start.9 = (bf16[128,2048]{1,0:T(8,128)(2,1)S(1)}, bf16[128,2048]{1,0:T(8,128)(2,1)}, u32[]{:S(2)}) copy-start(bf16[128,2048]{1,0:T(8,128)(2,1)} %residual.1) | copy-start | bytes 1572868
  43.3 30.3 %copy-start.27 = (f32[2048]{0:T(1024)S(1)}, f32[2048]{0:T(1024)}, u32[]{:S(2)}) copy-start(f32[2048]{0:T(1024)} %param.24) | copy-start | bytes 24580
  43.3 30.3 %copy-start.28 = (f32[2048]{0:T(1024)S(1)}, f32[2048]{0:T(1024)}, u32[]{:S(2)}) copy-start(f32[2048]{0:T(1024)} %param.25) | copy-start | bytes 24580
  43.3 28.3 %collective-permute-start.6 = (bf16[128,2048]{1,0:T(8,128)(2,1)S(1)}, bf16[128,2048]{1,0:T(8,128)(2,1)S(1)}, u32[]{:S(2)}, u32[]{:S(2)}) collective-permute-start(bf16[128,2048]{1,0:T(8,128)(2,1)S(1)} %shard_map.160), channel_id=1, source_target_pairs={{0,2},{1,3},{2,0},{3,1},{4,6},{5,7},{6,4},{7,5},{8,10},{9,11},{10,... | collective-permute-start | bytes 1572872 | tf_op jit(solution)/shard_map/ppermute | solution.py:420
  44.9 12.0 %collective-permute-start.19 = (bf16[256,768]{1,0:T(8,128)(2,1)S(1)}, bf16[256,768]{1,0:T(8,128)(2,1)S(1)}, u32[]{:S(2)}, u32[]{:S(2)}) collective-permute-start(bf16[256,768]{1,0:T(8,128)(2,1)S(1)} %copy-done.11), channel_id=1, source_target_pairs={{0,4},{4,0},{8,12},{12,8},{16,20},{20,16},{24,28},{28,24},{1,5},{5... | collective-permute-start | bytes 1179656 | tf_op jit(solution)/shard_map/ppermute | solution.py:430
  46.4 16.8 %collective-permute-start.20 = (bf16[256,768]{1,0:T(8,128)(2,1)S(1)}, bf16[256,768]{1,0:T(8,128)(2,1)S(1)}, u32[]{:S(2)}, u32[]{:S(2)}) collective-permute-start(bf16[256,768]{1,0:T(8,128)(2,1)S(1)} %copy-done.11), channel_id=1, source_target_pairs={{0,8},{4,12},{8,16},{12,20},{16,24},{20,28},{24,0},{28,4},{1,9},{5... | collective-permute-start | bytes 1179656 | tf_op jit(solution)/shard_map/ppermute | solution.py:426
  48.6 16.7 %collective-permute-start.26 = (bf16[256,768]{1,0:T(8,128)(2,1)S(1)}, bf16[256,768]{1,0:T(8,128)(2,1)S(1)}, u32[]{:S(2)}, u32[]{:S(2)}) collective-permute-start(bf16[256,768]{1,0:T(8,128)(2,1)S(1)} %copy-done.3), channel_id=1, source_target_pairs={{0,4},{4,0},{8,12},{12,8},{16,20},{20,16},{24,28},{28,24},{1,5},{5... | collective-permute-start | bytes 1179656 | tf_op jit(solution)/shard_map/ppermute | solution.py:430
  54.8 16.9 %collective-permute-start.27 = (bf16[256,768]{1,0:T(8,128)(2,1)S(1)}, bf16[256,768]{1,0:T(8,128)(2,1)S(1)}, u32[]{:S(2)}, u32[]{:S(2)}) collective-permute-start(bf16[256,768]{1,0:T(8,128)(2,1)S(1)} %copy-done.3), channel_id=1, source_target_pairs={{0,8},{4,12},{8,16},{12,20},{16,24},{20,28},{24,0},{28,4},{1,9},{5... | collective-permute-start | bytes 1179656 | tf_op jit(solution)/shard_map/ppermute | solution.py:426
  57.7 17.0 %collective-permute-start.14 = (bf16[256,768]{1,0:T(8,128)(2,1)S(1)}, bf16[256,768]{1,0:T(8,128)(2,1)S(1)}, u32[]{:S(2)}, u32[]{:S(2)}) collective-permute-start(bf16[256,768]{1,0:T(8,128)(2,1)S(1)} %collective-permute-done.13.refs_8_), channel_id=1, source_target_pairs={{0,4},{4,0},{8,12},{12,8},{16,20},{20,16},{24,28},{28,24},{1,5},{5... | collective-permute-start | bytes 1179656 | tf_op jit(solution)/shard_map/ppermute | solution.py:430
  63.2 10.4 %copy-start.15 = (bf16[256,768]{1,0:T(8,128)(2,1)}, bf16[256,768]{1,0:T(8,128)(2,1)S(1)}, u32[]{:S(2)}) copy-start(bf16[256,768]{1,0:T(8,128)(2,1)S(1)} %collective-permute-done.20.refs_2_) | copy-start | bytes 1179652
  63.2 17.0 %collective-permute-start.15 = (bf16[256,768]{1,0:T(8,128)(2,1)S(1)}, bf16[256,768]{1,0:T(8,128)(2,1)}, u32[]{:S(2)}, u32[]{:S(2)}) collective-permute-start(bf16[256,768]{1,0:T(8,128)(2,1)S(1)} %collective-permute-done.13.refs_8_), channel_id=1, source_target_pairs={{0,8},{4,12},{8,16},{12,20},{16,24},{20,28},{24,0},{28,4},{1,9},{5... | collective-permute-start | bytes 1179656 | tf_op jit(solution)/shard_map/ppermute | solution.py:426
  65.4 16.3 %collective-permute-start.21 = (bf16[256,768]{1,0:T(8,128)(2,1)S(1)}, bf16[256,768]{1,0:T(8,128)(2,1)S(1)}, u32[]{:S(2)}, u32[]{:S(2)}) collective-permute-start(bf16[256,768]{1,0:T(8,128)(2,1)S(1)} %collective-permute-done.20.refs_2_), channel_id=1, source_target_pairs={{0,4},{4,0},{8,12},{12,8},{16,20},{20,16},{24,28},{28,24},{1,5},{5... | collective-permute-start | bytes 1179656 | tf_op jit(solution)/shard_map/ppermute | solution.py:430
  71.6 17.0 %collective-permute-start.22 = (bf16[256,768]{1,0:T(8,128)(2,1)S(1)}, bf16[256,768]{1,0:T(8,128)(2,1)}, u32[]{:S(2)}, u32[]{:S(2)}) collective-permute-start(bf16[256,768]{1,0:T(8,128)(2,1)S(1)} %collective-permute-done.20.refs_2_), channel_id=1, source_target_pairs={{0,8},{4,12},{8,16},{12,20},{16,24},{20,28},{24,0},{28,4},{1,9},{5... | collective-permute-start | bytes 1179656 | tf_op jit(solution)/shard_map/ppermute | solution.py:426
  71.6 25.3 %collective-permute-start.28 = (bf16[256,768]{1,0:T(8,128)(2,1)S(1)}, bf16[256,768]{1,0:T(8,128)(2,1)S(1)}, u32[]{:S(2)}, u32[]{:S(2)}) collective-permute-start(bf16[256,768]{1,0:T(8,128)(2,1)S(1)} %collective-permute-done.27.refs_2_), channel_id=1, source_target_pairs={{0,8},{4,12},{8,16},{12,20},{16,24},{20,28},{24,0},{28,4},{1,9},{5... | collective-permute-start | bytes 1179656 | tf_op jit(solution)/shard_map/ppermute | solution.py:426
  75.5 39.9 %collective-permute-start.7 = (bf16[128,2048]{1,0:T(8,128)(2,1)S(1)}, bf16[128,2048]{1,0:T(8,128)(2,1)S(1)}, u32[]{:S(2)}, u32[]{:S(2)}) collective-permute-start(bf16[128,2048]{1,0:T(8,128)(2,1)S(1)} %get-tuple-element.40.refs_2_), channel_id=1, source_target_pairs={{0,1},{1,0},{2,3},{3,2},{4,5},{5,4},{6,7},{7,6},{8,9},{9,8},{10,11... | collective-permute-start | bytes 1572872 | tf_op jit(solution)/shard_map/ppermute | solution.py:419
  80.2 35.7 %collective-permute-start.10 = (bf16[128,2048]{1,0:T(8,128)(2,1)S(1)}, bf16[128,2048]{1,0:T(8,128)(2,1)S(1)}, u32[]{:S(2)}, u32[]{:S(2)}) collective-permute-start(bf16[128,2048]{1,0:T(8,128)(2,1)S(1)} %get-tuple-element.40.refs_2_), channel_id=1, source_target_pairs={{0,2},{1,3},{2,0},{3,1},{4,6},{5,7},{6,4},{7,5},{8,10},{9,11},{10,... | collective-permute-start | bytes 1572872 | tf_op jit(solution)/shard_map/ppermute | solution.py:420
  82.4 15.2 %collective-permute-start.16 = (bf16[256,768]{1,0:T(8,128)(2,1)}, bf16[256,768]{1,0:T(8,128)(2,1)}, u32[]{:S(2)}, u32[]{:S(2)}) collective-permute-start(bf16[256,768]{1,0:T(8,128)(2,1)} %collective-permute-done.15.refs_10_), channel_id=1, source_target_pairs={{0,4},{4,0},{8,12},{12,8},{16,20},{20,16},{24,28},{28,24},{1,5},{5... | collective-permute-start | bytes 1179656 | tf_op jit(solution)/shard_map/ppermute | solution.py:430
  88.6 16.9 %collective-permute-start.17 = (bf16[256,768]{1,0:T(8,128)(2,1)}, bf16[256,768]{1,0:T(8,128)(2,1)}, u32[]{:S(2)}, u32[]{:S(2)}) collective-permute-start(bf16[256,768]{1,0:T(8,128)(2,1)} %collective-permute-done.15.refs_10_), channel_id=1, source_target_pairs={{0,8},{4,12},{8,16},{12,20},{16,24},{20,28},{24,0},{28,4},{1,9},{5... | collective-permute-start | bytes 1179656 | tf_op jit(solution)/shard_map/ppermute | solution.py:426
  97.7 16.2 %collective-permute-start.24 = (bf16[256,768]{1,0:T(8,128)(2,1)}, bf16[256,768]{1,0:T(8,128)(2,1)}, u32[]{:S(2)}, u32[]{:S(2)}) collective-permute-start(bf16[256,768]{1,0:T(8,128)(2,1)} %collective-permute-done.22.refs_4_), channel_id=1, source_target_pairs={{0,8},{4,12},{8,16},{12,20},{16,24},{20,28},{24,0},{28,4},{1,9},{5... | collective-permute-start | bytes 1179656 | tf_op jit(solution)/shard_map/ppermute | solution.py:426
  97.7 47.2 %collective-permute-start.23 = (bf16[256,768]{1,0:T(8,128)(2,1)}, bf16[256,768]{1,0:T(8,128)(2,1)S(1)}, u32[]{:S(2)}, u32[]{:S(2)}) collective-permute-start(bf16[256,768]{1,0:T(8,128)(2,1)} %collective-permute-done.22.refs_4_), channel_id=1, source_target_pairs={{0,4},{4,0},{8,12},{12,8},{16,20},{20,16},{24,28},{28,24},{1,5},{5... | collective-permute-start | bytes 1179656 | tf_op jit(solution)/shard_map/ppermute | solution.py:430
  105.4 16.5 %collective-permute-start.32 = (bf16[256,768]{1,0:T(8,128)(2,1)}, bf16[256,768]{1,0:T(8,128)(2,1)S(1)}, u32[]{:S(2)}, u32[]{:S(2)}) collective-permute-start(bf16[256,768]{1,0:T(8,128)(2,1)} %copy-done.4), channel_id=1, source_target_pairs={{0,8},{4,12},{8,16},{12,20},{16,24},{20,28},{24,0},{28,4},{1,9},{5... | collective-permute-start | bytes 1179656 | tf_op jit(solution)/shard_map/ppermute | solution.py:426
  113.9 12.2 %collective-permute-start.18 = (bf16[256,768]{1,0:T(8,128)(2,1)}, bf16[256,768]{1,0:T(8,128)(2,1)S(1)}, u32[]{:S(2)}, u32[]{:S(2)}) collective-permute-start(bf16[256,768]{1,0:T(8,128)(2,1)} %collective-permute-done.17.refs_12_), channel_id=1, source_target_pairs={{0,4},{4,0},{8,12},{12,8},{16,20},{20,16},{24,28},{28,24},{1,5},{5... | collective-permute-start | bytes 1179656 | tf_op jit(solution)/shard_map/ppermute | solution.py:430
  115.4 29.6 %collective-permute-start.25 = (bf16[256,768]{1,0:T(8,128)(2,1)}, bf16[256,768]{1,0:T(8,128)(2,1)S(1)}, u32[]{:S(2)}, u32[]{:S(2)}) collective-permute-start(bf16[256,768]{1,0:T(8,128)(2,1)} %collective-permute-done.24.refs_6_), channel_id=1, source_target_pairs={{0,4},{4,0},{8,12},{12,8},{16,20},{20,16},{24,28},{28,24},{1,5},{5... | collective-permute-start | bytes 1179656 | tf_op jit(solution)/shard_map/ppermute | solution.py:430
  115.9 21.8 %collective-permute-start.11 = (bf16[128,2048]{1,0:T(8,128)(2,1)S(1)}, bf16[128,2048]{1,0:T(8,128)(2,1)S(1)}, u32[]{:S(2)}, u32[]{:S(2)}) collective-permute-start(bf16[128,2048]{1,0:T(8,128)(2,1)S(1)} %collective-permute-done.10.refs_4_), channel_id=1, source_target_pairs={{0,1},{1,0},{2,3},{3,2},{4,5},{5,4},{6,7},{7,6},{8,9},{9,8},{10,11... | collective-permute-start | bytes 1572872 | tf_op jit(solution)/shard_map/ppermute | solution.py:419
  115.9 29.0 %copy-start.25 = (f32[3,768]{1,0:T(4,128)S(1)}, f32[3,768]{1,0:T(4,128)}, u32[]{:S(2)}) copy-start(f32[3,768]{1,0:T(4,128)} %gate_taps.1) | copy-start | bytes 27652
  115.9 29.0 %copy-start.26 = (f32[3,768]{1,0:T(4,128)S(1)}, f32[3,768]{1,0:T(4,128)}, u32[]{:S(2)}) copy-start(f32[3,768]{1,0:T(4,128)} %value_taps.1) | copy-start | bytes 27652
  115.9 29.0 %copy-start.12 = (bf16[256,768]{1,0:T(8,128)(2,1)S(1)}, bf16[256,768]{1,0:T(8,128)(2,1)}, u32[]{:S(2)}) copy-start(bf16[256,768]{1,0:T(8,128)(2,1)} %refs_0_.3) | copy-start | bytes 1179652
  116.0 29.0 %copy-start.14 = (bf16[256,768]{1,0:T(8,128)(2,1)S(1)}, bf16[256,768]{1,0:T(8,128)(2,1)}, u32[]{:S(2)}) copy-start(bf16[256,768]{1,0:T(8,128)(2,1)} %copy-done.13) | copy-start | bytes 1179652
  116.0 29.0 %copy-start.16 = (bf16[256,768]{1,0:T(8,128)(2,1)S(1)}, bf16[256,768]{1,0:T(8,128)(2,1)}, u32[]{:S(2)}) copy-start(bf16[256,768]{1,0:T(8,128)(2,1)} %copy-done.15) | copy-start | bytes 1179652
  116.0 29.0 %copy-start.18 = (bf16[256,768]{1,0:T(8,128)(2,1)S(1)}, bf16[256,768]{1,0:T(8,128)(2,1)}, u32[]{:S(2)}) copy-start(bf16[256,768]{1,0:T(8,128)(2,1)} %copy-done.17) | copy-start | bytes 1179652
  121.9 4.8 %collective-permute-start.8 = (bf16[16,2048]{1,0:T(8,128)(2,1)S(1)}, bf16[16,2048]{1,0:T(8,128)(2,1)S(1)}, u32[]{:S(2)}, u32[]{:S(2)}) collective-permute-start(bf16[16,2048]{1,0:T(8,128)(2,1)S(1)} %slice_select_fusion), channel_id=1, source_target_pairs={{2,4},{3,5},{6,8},{7,9},{10,12},{11,13},{14,16},{15,17},{18,20},{1... | collective-permute-start | bytes 196616 | tf_op jit(solution)/shard_map/ppermute | solution.py:500
  126.1 3.3 %collective-permute-start.9 = (bf16[16,2048]{1,0:T(8,128)(2,1)S(1)}, bf16[16,2048]{1,0:T(8,128)(2,1)S(1)}, u32[]{:S(2)}, u32[]{:S(2)}) collective-permute-start(bf16[16,2048]{1,0:T(8,128)(2,1)S(1)} %slice_select_fusion), channel_id=1, source_target_pairs={{2,6},{3,7},{6,10},{7,11},{10,14},{11,15},{14,18},{15,19},{18,22},... | collective-permute-start | bytes 196616 | tf_op jit(solution)/shard_map/ppermute | solution.py:500
  126.7 25.2 %collective-permute-start.34 = (bf16[256,768]{1,0:T(8,128)(2,1)S(1)}, bf16[256,768]{1,0:T(8,128)(2,1)S(1)}, u32[]{:S(2)}, u32[]{:S(2)}) collective-permute-start(bf16[256,768]{1,0:T(8,128)(2,1)S(1)} %collective-permute-done.26.refs_1_), channel_id=1, source_target_pairs={{0,8},{4,12},{8,16},{12,20},{16,24},{20,28},{24,0},{28,4},{1,9},{5... | collective-permute-start | bytes 1179656 | tf_op jit(solution)/shard_map/ppermute | solution.py:428
  129.4 22.6 %collective-permute-start.33 = (bf16[256,768]{1,0:T(8,128)(2,1)}, bf16[256,768]{1,0:T(8,128)(2,1)S(1)}, u32[]{:S(2)}, u32[]{:S(2)}) collective-permute-start(bf16[256,768]{1,0:T(8,128)(2,1)} %copy-done.4), channel_id=1, source_target_pairs={{0,4},{4,0},{8,12},{12,8},{16,20},{20,16},{24,28},{28,24},{1,5},{5... | collective-permute-start | bytes 1179656 | tf_op jit(solution)/shard_map/ppermute | solution.py:430
  137.7 19.0 %collective-permute-start.38 = (bf16[256,768]{1,0:T(8,128)(2,1)S(1)}, bf16[256,768]{1,0:T(8,128)(2,1)S(1)}, u32[]{:S(2)}, u32[]{:S(2)}) collective-permute-start(bf16[256,768]{1,0:T(8,128)(2,1)S(1)} %collective-permute-done.32.refs_0_), channel_id=1, source_target_pairs={{0,4},{4,0},{8,12},{12,8},{16,20},{20,16},{24,28},{28,24},{1,5},{5... | collective-permute-start | bytes 1179656 | tf_op jit(solution)/shard_map/ppermute | solution.py:430
  145.0 5.7 %copy-start.5 = (bf16[256,768]{1,0:T(8,128)(2,1)S(1)}, bf16[256,768]{1,0:T(8,128)(2,1)}, u32[]{:S(2)}) copy-start(bf16[256,768]{1,0:T(8,128)(2,1)} %copy-done.4) | copy-start | bytes 1179652
  151.9 2.9 %collective-permute-start.29 = (bf16[128,1024]{1,0:T(8,128)(2,1)S(1)}, bf16[128,1024]{1,0:T(8,128)(2,1)S(1)}, u32[]{:S(2)}, u32[]{:S(2)}) collective-permute-start(bf16[128,1024]{1,0:T(8,128)(2,1)S(1)} %get-tuple-element.46), channel_id=1, source_target_pairs={{0,1},{1,0},{2,3},{3,2},{4,5},{5,4},{6,7},{7,6},{8,9},{9,8},{10,11... | collective-permute-start | bytes 786440 | tf_op jit(solution)/shard_map/ppermute | solution.py:419
  153.0 6.6 %collective-permute-start.35 = (bf16[128,768]{1,0:T(8,128)(2,1)S(1)}, bf16[128,768]{1,0:T(8,128)(2,1)S(1)}, u32[]{:S(2)}, u32[]{:S(2)}) collective-permute-start(bf16[128,768]{1,0:T(8,128)(2,1)S(1)} %get-tuple-element.50), channel_id=1, source_target_pairs={{0,1},{1,0},{2,3},{3,2},{4,5},{5,4},{6,7},{7,6},{8,9},{9,8},{10,11... | collective-permute-start | bytes 589832 | tf_op jit(solution)/shard_map/ppermute | solution.py:419
  154.7 17.3 %collective-permute-start.31 = (bf16[128,1024]{1,0:T(8,128)(2,1)S(1)}, bf16[128,1024]{1,0:T(8,128)(2,1)S(1)}, u32[]{:S(2)}, u32[]{:S(2)}) collective-permute-start(bf16[128,1024]{1,0:T(8,128)(2,1)S(1)} %get-tuple-element.48), channel_id=1, source_target_pairs={{0,1},{1,0},{2,3},{3,2},{4,5},{5,4},{6,7},{7,6},{8,9},{9,8},{10,11... | collective-permute-start | bytes 786440 | tf_op jit(solution)/shard_map/ppermute | solution.py:419
  155.4 16.6 %collective-permute-start.30 = (bf16[128,1024]{1,0:T(8,128)(2,1)S(1)}, bf16[128,1024]{1,0:T(8,128)(2,1)S(1)}, u32[]{:S(2)}, u32[]{:S(2)}) collective-permute-start(bf16[128,1024]{1,0:T(8,128)(2,1)S(1)} %shard_map.166), channel_id=1, source_target_pairs={{0,2},{1,3},{2,0},{3,1},{4,6},{5,7},{6,4},{7,5},{8,10},{9,11},{10,... | collective-permute-start | bytes 786440 | tf_op jit(solution)/shard_map/ppermute | solution.py:547
  157.5 14.5 %copy-start.29 = (f32[2048]{0:T(1024)S(1)}, f32[2048]{0:T(1024)}, u32[]{:S(2)}) copy-start(f32[2048]{0:T(1024)} %param.31) | copy-start | bytes 24580
  157.6 8.5 %collective-permute-start.39 = (bf16[128,256]{1,0:T(8,128)(2,1)S(1)}, bf16[128,256]{1,0:T(8,128)(2,1)S(1)}, u32[]{:S(2)}, u32[]{:S(2)}) collective-permute-start(bf16[128,256]{1,0:T(8,128)(2,1)S(1)} %get-tuple-element.53), channel_id=1, source_target_pairs={{0,2},{1,3},{2,0},{3,1},{4,6},{5,7},{6,4},{7,5},{8,10},{9,11},{10,... | collective-permute-start | bytes 196616 | tf_op jit(solution)/shard_map/ppermute | solution.py:541
  159.5 12.5 %collective-permute-start.37 = (bf16[128,768]{1,0:T(8,128)(2,1)S(1)}, bf16[128,768]{1,0:T(8,128)(2,1)S(1)}, u32[]{:S(2)}, u32[]{:S(2)}) collective-permute-start(bf16[128,768]{1,0:T(8,128)(2,1)S(1)} %get-tuple-element.52), channel_id=1, source_target_pairs={{0,1},{1,0},{2,3},{3,2},{4,5},{5,4},{6,7},{7,6},{8,9},{9,8},{10,11... | collective-permute-start | bytes 589832 | tf_op jit(solution)/shard_map/ppermute | solution.py:419
  160.2 11.8 %collective-permute-start.36 = (bf16[128,768]{1,0:T(8,128)(2,1)S(1)}, bf16[128,768]{1,0:T(8,128)(2,1)S(1)}, u32[]{:S(2)}, u32[]{:S(2)}) collective-permute-start(bf16[128,768]{1,0:T(8,128)(2,1)S(1)} %shard_map.169), channel_id=1, source_target_pairs={{0,2},{1,3},{2,0},{3,1},{4,6},{5,7},{6,4},{7,5},{8,10},{9,11},{10,... | collective-permute-start | bytes 589832 | tf_op jit(solution)/shard_map/ppermute | solution.py:547
  166.1 4.6 %collective-permute-start.40 = (bf16[128,256]{1,0:T(8,128)(2,1)S(1)}, bf16[128,256]{1,0:T(8,128)(2,1)S(1)}, u32[]{:S(2)}, u32[]{:S(2)}) collective-permute-start(bf16[128,256]{1,0:T(8,128)(2,1)S(1)} %get-tuple-element.54), channel_id=1, source_target_pairs={{0,3},{1,2},{2,1},{3,0},{4,7},{5,6},{6,5},{7,4},{8,11},{9,10},{10,... | collective-permute-start | bytes 196616 | tf_op jit(solution)/shard_map/ppermute | solution.py:542
  170.7 1.3 collective-permute-start.41
  (13 other events, 10.9 us)
